TPU v7x, 32 devices: a whole 2x2x4 slice. The times are simulated.
32 devices in a mesh: fs: 4 (over z), rep: 4 (over y, x), tp: 2 (over core).
Axes of the slice: x: 2, y: 2, z: 4, core: 2. Of those that a mesh axis runs over, the one named last changes fastest.
Arguments:
- inputs: bfloat16 [2048, 2048], P(('fs', 'rep')), may hold values from -6 to 6
- query_cot: bfloat16 [2048, 1024], P(('fs', 'rep'), 'tp'), may hold values from -0.125 to 0.125
- attended: bfloat16 [2048, 1024], P(('fs', 'rep')), may hold values from -6 to 6
- output_cot: bfloat16 [2048, 2048], P(('fs', 'rep'), 'tp'), may hold values from -0.125 to 0.125
- proj_query: bfloat16 [2048, 256], P('fs'), may hold values from -0.125 to 0.125
- proj_output: bfloat16 [1024, 256], P('fs'), may hold values from -0.1875 to 0.1875
- weight_query: float32 [2048, 1024], P('fs', 'tp'), may hold values from -0.125 to 0.125
- weight_output: float32 [1024, 2048], P('fs', 'tp'), may hold values from -0.1875 to 0.1875
- first_query: float32 [256, 1024], P('fs', 'tp'), may hold values from -6 to 6
- second_query: float32 [256, 1024], P('fs', 'tp'), may hold values from 0.0002 to 2
- first_output: float32 [256, 2048], P('fs', 'tp'), may hold values from -6 to 6
- second_output: float32 [256, 2048], P('fs', 'tp'), may hold values from 0.0002 to 2
Outputs:
- new_weight_query: float32 [2048, 1024], P('fs', 'tp')
- new_weight_output: float32 [1024, 2048], P('fs', 'tp')
- step_query: float32 [2048, 1024], P('fs', 'tp')
- step_output: float32 [1024, 2048], P('fs', 'tp')
- new_first_query: float32 [256, 1024], P('fs', 'tp')
- new_second_query: float32 [256, 1024], P('fs', 'tp')
- new_first_output: float32 [256, 2048], P('fs', 'tp')
- new_second_output: float32 [256, 2048], P('fs', 'tp')
- copy_query: bfloat16 [2048, 1024], P(None, 'tp')
- copy_output: bfloat16 [1024, 2048], P(None, 'tp')
All inputs are finite; a program needn't handle non-finite values.
Results may differ from a plain program's by a relative error of at most 0.0031.
Values may be sent and summed in bfloat16 or wider, within the bound.
A program may use at most 64 MiB of HBM per device.

v0:
```python
import functools

import jax
import jax.numpy as jnp
from jax import lax
from jax.experimental import pallas as pl
from jax.experimental.pallas import tpu as pltpu
from jax.sharding import PartitionSpec as P

beta_first = 0.9
beta_second = 0.95
adam_eps = 1e-08
mean_eps = 1e-06
learn_rate = 0.02

MESH = pl.DeviceIdType.MESH
F32 = jnp.float32
BF16 = jnp.bfloat16


def kernel(
    n, r, tp, entries,
    x_ref, qc_ref, a_ref, oc_ref, pq_ref, po_ref, wq_ref, wo_ref, fq_ref, sq_ref, fo_ref, so_ref,
    nwq, nwo, stq, sto, nfq, nsq, nfo, nso, cpq, cpo,
    allq, allo, allx, alla, allqc, alloc, sbuf, r2, lowg, half, tz, tr, tt,
    pz_s, pz_r, pt_s, pt_r, xr_s, xr_r, xt_s, xt_r, cr1_s, cr1_r, r2_s, r2_r, lg_s, lg_r, hz_s, hz_r, hr_s, hr_r,
    tz_s, tz_r, tr_s, tr_r, tt_s, tt_r, cz_s, cz_r, cr_s, cr_r,
):
    f, k, t = lax.axis_index("fs"), lax.axis_index("rep"), lax.axis_index("tp")
    other = {"tp": 1 - t}
    rows_q, rank = pq_ref.shape
    rows_o = po_ref.shape[0]
    low_rows = fq_ref.shape[0]
    quarter_q, quarter_o = fq_ref.shape[1] // r, fo_ref.shape[1] // r
    fs_peers = [lax.rem(f + d, n) for d in range(1, n)]
    rep_peers = [lax.rem(k + d, r) for d in range(1, r)]
    from_fs, from_rep = fs_peers[::-1], rep_peers[::-1]
    across = r == 4
    if across:
        near, far = k + 1 - 2 * lax.rem(k, 2), lax.rem(k + 2, r)
        beyond = lax.rem(near + 2, r)
        targets = [near, far]
    else:
        targets = rep_peers

    def send(src, dst, ssem, rsem, where):
        copy = pltpu.make_async_remote_copy(
            src_ref=src, dst_ref=dst, send_sem=ssem, recv_sem=rsem, device_id=where, device_id_type=MESH
        )
        copy.start()
        return copy

    def arrived(dst, ssem, rsem, where):
        pltpu.make_async_remote_copy(
            src_ref=dst, dst_ref=dst, send_sem=ssem, recv_sem=rsem, device_id=where, device_id_type=MESH
        ).wait_recv()

    def cols(index, width):
        return pl.ds(pl.multiple_of(index * width, width), width)

    barrier = pltpu.get_barrier_semaphore()
    for j in fs_peers:
        pl.semaphore_signal(barrier, inc=1, device_id={"fs": j}, device_id_type=MESH)
    for j in rep_peers:
        pl.semaphore_signal(barrier, inc=1, device_id={"rep": j}, device_id_type=MESH)
    pl.semaphore_signal(barrier, inc=1, device_id=other, device_id_type=MESH)
    pl.semaphore_wait(barrier, n - 1 + r - 1 + 1)

    sent = []
    tokens = x_ref.shape[0]
    pieces = ((pq_ref, allq, rows_q // tp, 0), (po_ref, allo, rows_o // tp, 1))
    loads = ((x_ref, allx, tokens // tp, 0), (a_ref, alla, tokens // tp, 1))
    for j in fs_peers:
        for own, whole, part, i in pieces:
            mine = cols(t, part)
            sent.append(send(own.at[mine], whole.at[f, mine], pz_s.at[i, j], pz_r.at[i, f], {"fs": j}))
    for j in targets:
        for own, whole, part, i in loads:
            mine = cols(t, part)
            sent.append(send(own.at[mine], whole.at[k, mine], xr_s.at[i, j], xr_r.at[i, k], {"rep": j}))
    for j in rep_peers:
        for own, whole, width, i in ((qc_ref, allqc, quarter_q, 0), (oc_ref, alloc, quarter_o, 1)):
            sent.append(send(own.at[:, cols(j, width)], whole.at[k], cr1_s.at[i, j], cr1_r.at[i, k], {"rep": j}))
    allq[f] = pq_ref[...]
    allo[f] = po_ref[...]
    allx[k] = x_ref[...]
    alla[k] = a_ref[...]
    allqc[k] = qc_ref[:, cols(k, quarter_q)]
    alloc[k] = oc_ref[:, cols(k, quarter_o)]
    def hand_over(group, j, s1, r1, s2, r2_, axis):
        for own, whole, part, i in group:
            mine = cols(t, part)
            arrived(whole.at[j, mine], s1.at[i, j], r1.at[i, j], {axis: j})
            sent.append(send(whole.at[j, mine], whole.at[j, mine], s2.at[i, j], r2_.at[i, j], other))

    def half_rows(part, which):
        return cols(2 * t + which, part // 2)

    def pass_on(source, to, which):
        for own, whole, part, i in loads:
            rows = half_rows(part, which)
            block = whole.at[source, rows]
            sent.append(send(block, block, xr_s.at[i + 2 * which, beyond], xr_r.at[i + 2 * which, source], {"rep": to}))

    if across:
        for which, (source, to) in enumerate(((near, far), (far, near))):
            hand_over(loads, source, xr_s, xr_r, xt_s, xt_r, "rep")
            pass_on(source, to, which)
    else:
        for j in from_rep:
            hand_over(loads, j, xr_s, xr_r, xt_s, xt_r, "rep")
    for j in from_fs:
        hand_over(pieces, j, pz_s, pz_r, pt_s, pt_r, "fs")
    if across:
        for own, whole, part, i in loads:
            for which in range(2):
                block = whole.at[beyond, half_rows(part, which)]
                at = i + 2 * which
                arrived(block, xr_s.at[at, beyond], xr_r.at[at, beyond], {"rep": beyond})
                sent.append(send(block, block, xt_s.at[at, beyond], xt_r.at[at, beyond], other))
    for peers, group, s2, r2_ in ((fs_peers, pieces, pt_s, pt_r), (targets, loads, xt_s, xt_r)):
        for j in peers:
            for own, whole, part, i in group:
                arrived(whole.at[j, cols(1 - t, part)], s2.at[i, j], r2_.at[i, j], other)
    if across:
        for own, whole, part, i in loads:
            for which in range(2):
                block = whole.at[beyond, cols(2 * (1 - t) + which, part // 2)]
                at = i + 2 * which
                arrived(block, xt_s.at[at, beyond], xt_r.at[at, beyond], other)
    for j in rep_peers:
        for whole, i in ((allqc, 0), (alloc, 1)):
            arrived(whole.at[j], cr1_s.at[i, j], cr1_r.at[i, j], {"rep": j})

    def projected(load, factor, cot):
        load, factor, cot = (v[...].reshape(-1, v.shape[-1]) for v in (load, factor, cot))
        turned = jnp.dot(load, factor, preferred_element_type=F32).T
        high = turned.astype(BF16)
        rest = (turned - high.astype(F32)).astype(BF16)
        return jnp.dot(high, cot, preferred_element_type=F32) + jnp.dot(rest, cot, preferred_element_type=F32)

    total_q = projected(allx, allq, allqc)
    total_o = projected(alla, allo, alloc)
    sbuf[:, :, :quarter_q] = total_q.reshape(n, low_rows, quarter_q)
    sbuf[:, :, quarter_q:] = total_o.reshape(n, low_rows, quarter_o)
    for j in fs_peers:
        sent.append(send(sbuf.at[j], r2.at[f], r2_s.at[j], r2_r.at[f], {"fs": j}))
    low = sbuf[f]
    for j in fs_peers:
        arrived(r2.at[j], r2_s.at[j], r2_r.at[j], {"fs": j})
        low += r2[j]
    lowg[k] = low

    def update(low_sum, first, second):
        first_new = beta_first * first + (1.0 - beta_first) * low_sum
        second_new = beta_second * second + (1.0 - beta_second) * low_sum * low_sum
        return first_new, second_new, first_new / (jnp.sqrt(second_new) + adam_eps)

    at_q, at_o = cols(k, quarter_q), cols(k, quarter_o)
    normed_q = update(low[:, :quarter_q], fq_ref[:, at_q], sq_ref[:, at_q])[2]
    normed_o = update(low[:, quarter_q:], fo_ref[:, at_o], so_ref[:, at_o])[2]
    half[k, f, :, :quarter_q] = normed_q.astype(BF16)
    half[k, f, :, quarter_q:] = normed_o.astype(BF16)
    share = jnp.sum(normed_q * normed_q) + jnp.sum(normed_o * normed_o)
    tz[f] = jnp.full(tz.shape[1:], share, F32)
    for j in fs_peers:
        sent.append(send(tz.at[f], tz.at[f], tz_s.at[j], tz_r.at[f], {"fs": j}))
        sent.append(send(half.at[k, f], half.at[k, f], hz_s.at[j], hz_r.at[f], {"fs": j}))
    for j in rep_peers:
        sent.append(send(half.at[k, f], half.at[k, f], hr_s.at[f, j], hr_r.at[f, k], {"rep": j}))

    for j in fs_peers:
        arrived(tz.at[j], tz_s.at[j], tz_r.at[j], {"fs": j})
    tr[k] = jnp.sum(tz[...], axis=0)
    for j in rep_peers:
        sent.append(send(tr.at[k], tr.at[k], tr_s.at[j], tr_r.at[k], {"rep": j}))
    for j in from_fs:
        arrived(half.at[k, j], hz_s.at[j], hz_r.at[j], {"fs": j})
        for m in rep_peers:
            sent.append(send(half.at[k, j], half.at[k, j], hr_s.at[j, m], hr_r.at[j, k], {"rep": m}))
    for j in rep_peers:
        arrived(tr.at[j], tr_s.at[j], tr_r.at[j], {"rep": j})
    tt[t] = jnp.sum(tr[...], axis=0)
    sent.append(send(tt.at[t], tt.at[t], tt_s.at[0], tt_r.at[0], other))

    def weights(index, scale):
        block = half[index].reshape(rank, quarter_q + quarter_o)
        for proj, lo, hi, width, old, new, step, copy, rows in (
            (pq_ref, 0, quarter_q, quarter_q, wq_ref, nwq, stq, cpq, rows_q),
            (po_ref, quarter_q, quarter_q + quarter_o, quarter_o, wo_ref, nwo, sto, cpo, rows_o),
        ):
            at = cols(index, width)
            moved = scale * jnp.dot(proj[...], block[:, lo:hi], preferred_element_type=F32)
            fresh = old[:, at] - learn_rate * moved
            step[:, at] = moved
            new[:, at] = fresh
            copy[cols(f, rows), at] = fresh.astype(BF16)

    arrived(tt.at[1 - t], tt_s.at[0], tt_r.at[0], other)
    scale = lax.rsqrt((tt[0] + tt[1])[:1, :1] / entries + mean_eps)
    weights(k, scale)
    outs = ((cpq, rows_q, quarter_q, 0), (cpo, rows_o, quarter_o, 1))
    for j in fs_peers:
        for copy, rows, width, i in outs:
            block = copy.at[cols(f, rows), cols(k, width)]
            sent.append(send(block, block, cz_s.at[i, j], cz_r.at[i, f], {"fs": j}))
    for j in rep_peers:
        sent.append(send(lowg.at[k], lowg.at[k], lg_s.at[j], lg_r.at[k], {"rep": j}))
    for m in from_rep:
        for j in [f] + from_fs:
            arrived(half.at[m, j], hr_s.at[j, m], hr_r.at[j, m], {"rep": m})
        weights(m, scale)
    def block_of(i, j, m):
        copy, rows, width, _ = outs[i]
        return copy.at[cols(j, rows), cols(m, width)]

    def relay(j):
        for i, source, to in ((0, near, far), (1, far, near)):
            block = block_of(i, j, source)
            arrived(block, cr_s.at[i, j, source], cr_r.at[i, j, source], {"rep": source})
            sent.append(send(block, block, cr_s.at[i, j, beyond], cr_r.at[i, j, source], {"rep": to}))

    for step, j in enumerate(from_fs):
        for i in range(2):
            block = block_of(i, j, k)
            arrived(block, cz_s.at[i, j], cz_r.at[i, j], {"fs": j})
            for m in targets:
                sent.append(send(block, block, cr_s.at[i, j, m], cr_r.at[i, j, k], {"rep": m}))
        if across and step:
            relay(from_fs[step - 1])
    if across and from_fs:
        relay(from_fs[-1])
    for m in [k] + rep_peers:
        if m is not k:
            arrived(lowg.at[m], lg_s.at[m], lg_r.at[m], {"rep": m})
        block = lowg[m]
        at_q, at_o = cols(m, quarter_q), cols(m, quarter_o)
        nfq[:, at_q], nsq[:, at_q], _ = update(block[:, :quarter_q], fq_ref[:, at_q], sq_ref[:, at_q])
        nfo[:, at_o], nso[:, at_o], _ = update(block[:, quarter_q:], fo_ref[:, at_o], so_ref[:, at_o])
    late = ((1, near), (0, far), (0, beyond), (1, beyond)) if across else [(i, m) for m in from_rep for i in range(2)]
    for j in from_fs:
        for i, m in late:
            arrived(block_of(i, j, m), cr_s.at[i, j, m], cr_r.at[i, j, m], {"rep": m})
    for copy in sent:
        copy.wait_send()


def place(*refs):
    count = len(refs) // 2
    sems = refs[-1]
    copies = [pltpu.make_async_copy(refs[i], refs[count + i], sems.at[i]) for i in range(count)]
    for copy in copies:
        copy.start()
    for copy in copies:
        copy.wait()


def solution(mesh):
    n, r, tp = mesh.shape["fs"], mesh.shape["rep"], mesh.shape["tp"]

    def local(*args):
        x, qc, a, oc, pq, po, wq, wo, fq, sq, fo, so = args
        rank = pq.shape[1]
        low_rows = fq.shape[0]
        wide = (fq.shape[1] + fo.shape[1]) // r
        entries = rank * (fq.shape[1] + fo.shape[1]) * tp
        shape = jax.ShapeDtypeStruct
        like = lambda v: shape(v.shape, v.dtype)
        dma = pltpu.SemaphoreType.DMA
        made = pl.pallas_call(
            functools.partial(kernel, n, r, tp, entries),
            out_shape=(
                like(wq), like(wo), like(wq), like(wo), like(fq), like(sq), like(fo), like(so),
                shape((n * wq.shape[0], wq.shape[1]), BF16),
                shape((n * wo.shape[0], wo.shape[1]), BF16),
            ),
            in_specs=[pl.BlockSpec(memory_space=pltpu.VMEM)] * 12,
            out_specs=[pl.BlockSpec(memory_space=pltpu.VMEM)] * 10,
            scratch_shapes=[
                pltpu.VMEM((n,) + pq.shape, BF16),
                pltpu.VMEM((n,) + po.shape, BF16),
                pltpu.VMEM((r,) + x.shape, BF16),
                pltpu.VMEM((r,) + a.shape, BF16),
                pltpu.VMEM((r, qc.shape[0], qc.shape[1] // r), BF16),
                pltpu.VMEM((r, oc.shape[0], oc.shape[1] // r), BF16),
                pltpu.VMEM((n, low_rows, wide), F32),
                pltpu.VMEM((n, low_rows, wide), F32),
                pltpu.VMEM((r, low_rows, wide), F32),
                pltpu.VMEM((r, n, low_rows, wide), BF16),
                pltpu.VMEM((n, 8, 128), F32),
                pltpu.VMEM((r, 8, 128), F32),
                pltpu.VMEM((tp, 8, 128), F32),
                dma((2, n)), dma((2, n)), dma((2, n)), dma((2, n)),
                dma((4, r)), dma((4, r)), dma((4, r)), dma((4, r)), dma((2, r)), dma((2, r)), dma((n,)), dma((n,)), dma((r,)), dma((r,)),
                dma((n,)), dma((n,)), dma((n, r)), dma((n, r)),
                dma((n,)), dma((n,)), dma((r,)), dma((r,)), dma((1,)), dma((1,)),
                dma((2, n)), dma((2, n)), dma((2, n, r)), dma((2, n, r)),
            ],
            compiler_params=pltpu.CompilerParams(collective_id=0, has_side_effects=True),
        )(*args)
        return pl.pallas_call(
            place,
            out_shape=tuple(like(v) for v in made),
            in_specs=[pl.BlockSpec(memory_space=pltpu.VMEM)] * len(made),
            out_specs=[pl.BlockSpec(memory_space=pl.ANY)] * len(made),
            scratch_shapes=[dma((len(made),))],
        )(*made)

    both, rows = P(("fs", "rep"), "tp"), P("fs", "tp")
    whole = P(("fs", "rep"), None)
    return jax.shard_map(
        local,
        mesh=mesh,
        in_specs=(whole, both, whole, both, P("fs", None), P("fs", None)) + (rows,) * 6,
        out_specs=(rows,) * 8 + (P(None, "tp"),) * 2,
        check_vma=False,
    )
```

profile of v0, /device:TPU:25, one launch (start us, length us, event | category | flops | bytes accessed | tf_op | source)
XLA Modules:
  0.0 103.4 jit_solution(13585069492952552160)
XLA Ops:
  0.6 95.3 %shard_map.195 = (f32[512,512]{1,0:T(8,128)}, f32[256,1024]{1,0:T(8,128)}, f32[512,512]{1,0:T(8,128)}, f32[256,1024]{1,0:T(8,128)}, f32[64,512]{1,0:T(8,128)}, /...) custom-call(bf16[128,2048]{1,0:T(8,128)(2,1)} %x_ref.1, ...), custom_call_target="tpu_custom_call" | custom-call | tf_op jit(solution)/shard_map/pallas_call | solution.py:270
  96.0 7.4 %shard_map.196 = (f32[512,512]{1,0:T(8,128)}, f32[256,1024]{1,0:T(8,128)}, f32[512,512]{1,0:T(8,128)}, f32[256,1024]{1,0:T(8,128)}, f32[64,512]{1,0:T(8,128)}, /...) custom-call(f32[512,512]{1,0:T(8,128)} %get-tuple-element.20.refs_0_, ...), custom_call_target="tpu_custom_call" | custom-call | tf_op jit(solution)/shard_map/pallas_call | solution.py:301
where the time goes:
time: 104 us; the launch traced here: 103 us
  Pallas kernels  103 us (99%)
    pallas_call x1, Pallas kernels, local(): pl.pallas_call(functools.partial(kernel, n, r, tp, entries), out_shape=(l...  95.3 us
    pallas_call x1, Pallas kernels, local(): pl.pallas_call(place, out_shape=tuple((like(v) for v in made)), in_specs=...  7.37 us

commit v1 on v0

v1 whole, which is shorter than its diff:
```python
import functools

import jax
import jax.numpy as jnp
from jax import lax
from jax.experimental import pallas as pl
from jax.experimental.pallas import tpu as pltpu
from jax.sharding import PartitionSpec as P

beta_first = 0.9
beta_second = 0.95
adam_eps = 1e-08
mean_eps = 1e-06
learn_rate = 0.02

MESH = pl.DeviceIdType.MESH
F32 = jnp.float32
BF16 = jnp.bfloat16


def kernel(
    n, r, tp, entries, parts, xparts,
    x_h, qc_h, a_h, oc_h, pq_h, po_h, wq_h, wo_h, fq_h, sq_h, fo_h, so_h,
    nwq, nwo, stq, sto, nfq, nsq, nfo, nso, cpq, cpo,
    allq, allo, allx, alla, qcv, ocv, allqc, alloc, wqv, wov, fqv, sqv, fov, sov,
    sbq, sbo, r2q, r2o, lowgq, lowgo, halfq, halfo, tz,
    ld, po_s, po_r, pq_s, pq_r, pt_s, pt_r, ar_s, ar_r, at_s, at_r, xr_s, xr_r, xt_s, xt_r, cr1_s, cr1_r,
    r2_s, r2_r, lg_s, lg_r, hz_s, hz_r, hr_s, hr_r, tz_s, tz_r, cz_s, cz_r, cr_s, cr_r,
):
    f, k, t = lax.axis_index("fs"), lax.axis_index("rep"), lax.axis_index("tp")
    other = {"tp": 1 - t}
    total = n * r * tp
    me = (f * r + k) * tp + t
    rows_q, rank = pq_h.shape
    rows_o = po_h.shape[0]
    low_rows = fq_h.shape[0]
    tokens = x_h.shape[0]
    quarter_q, quarter_o = fq_h.shape[1] // r, fo_h.shape[1] // r
    fs_peers = [lax.rem(f + d, n) for d in range(1, n)]
    rep_peers = [lax.rem(k + d, r) for d in range(1, r)]
    from_fs, from_rep = fs_peers[::-1], rep_peers[::-1]
    across = r == 4
    if across:
        near, far = k + 1 - 2 * lax.rem(k, 2), lax.rem(k + 2, r)
        beyond = lax.rem(near + 2, r)
        targets = [near, far]
    else:
        targets = rep_peers
    sent = []

    def device(p):
        return {"fs": lax.div(p, r * tp), "rep": lax.rem(lax.div(p, tp), r), "tp": lax.rem(p, tp)}

    def remote(src, dst, ssem, rsem, where):
        return pltpu.make_async_remote_copy(
            src_ref=src, dst_ref=dst, send_sem=ssem, recv_sem=rsem, device_id=where, device_id_type=MESH
        )

    def run(cond, action):
        if cond is None:
            action()
        else:
            pl.when(cond)(action)

    def send(src, dst, ssem, rsem, where, cond=None):
        copy = remote(src, dst, ssem, rsem, where)
        run(cond, copy.start)
        sent.append((cond, copy))

    def arrived(dst, ssem, rsem, where, cond=None):
        run(cond, remote(dst, dst, ssem, rsem, where).wait_recv)

    def cols(index, width):
        return pl.ds(pl.multiple_of(index * width, width), width)

    barrier = pltpu.get_barrier_semaphore()

    def greet(i, carry):
        pl.semaphore_signal(barrier, inc=1, device_id=device(lax.rem(me + i, total)), device_id_type=MESH)
        return carry

    lax.fori_loop(1, total, greet, 0)

    loads = []

    def load(src, dst):
        copy = pltpu.make_async_copy(src, dst, ld.at[len(loads)])
        copy.start()
        loads.append(copy)
        return copy

    load_po = load(po_h, allo.at[f])
    load_a = load(a_h, alla.at[k])
    load_oc = load(oc_h, ocv)
    load_pq = load(pq_h, allq.at[f])
    load_qc = load(qc_h, qcv)
    load_x = load(x_h, allx.at[k])
    load_oc_own = load(oc_h.at[:, cols(k, quarter_o)], alloc.at[k])
    load_qc_own = load(qc_h.at[:, cols(k, quarter_q)], allqc.at[k])
    load_moments = [load(s, d) for s, d in ((fo_h, fov), (so_h, sov), (fq_h, fqv), (sq_h, sqv))]
    load_weights = [load(s, d) for s, d in ((wq_h, wqv), (wo_h, wov))]

    load_po.wait()
    load_a.wait()
    load_oc.wait()
    pl.semaphore_wait(barrier, total - 1)

    def half_rows(part, which):
        return cols(2 * t + which, part // 2)

    def sides(d):
        return (
            (f >= d, lax.rem(f + n - d, n), jnp.logical_and(f >= d, f < n - 1), lax.rem(f + 1, n), 0),
            (f + d < n, lax.rem(f + d, n), jnp.logical_and(f + d < n, f > 0), lax.rem(f + n - 1, n), 1),
        )

    outward = ((f < n - 1, lax.rem(f + 1, n), 0), (f > 0, lax.rem(f + n - 1, n), 1))

    part_po, part_pq, part_t = rows_o // tp, rows_q // tp, tokens // tp
    mine_po, mine_pq, mine_t = cols(t, part_po), cols(t, part_pq), cols(t, part_t)
    their_po, their_pq = cols(1 - t, part_po), cols(1 - t, part_pq)
    for j in fs_peers:
        block = allo.at[f, mine_po]
        send(block, block, po_s.at[j], po_r.at[f], {"fs": j})
    for j in targets:
        block = alla.at[k, mine_t]
        send(block, block, ar_s.at[0, j], ar_r.at[0, k], {"rep": j})
    for j in rep_peers:
        send(ocv.at[:, cols(j, quarter_o)], alloc.at[k], cr1_s.at[1, j], cr1_r.at[1, k], {"rep": j})
    load_pq.wait()
    for cond, to, way in outward:
        block = allq.at[f, mine_pq]
        send(block, block, pq_s.at[f, way], pq_r.at[f], {"fs": to}, cond)

    if across:
        for which, (source, to) in enumerate(((near, far), (far, near))):
            block = alla.at[source, mine_t]
            arrived(block, ar_s.at[0, source], ar_r.at[0, source], {"rep": source})
            rows = half_rows(part_t, which)
            piece = alla.at[source, rows]
            send(piece, piece, ar_s.at[1 + which, beyond], ar_r.at[1 + which, source], {"rep": to})
            send(block, block, at_s.at[0, source], at_r.at[0, source], other)
    load_qc.wait()
    load_x.wait()
    for j in rep_peers:
        send(qcv.at[:, cols(j, quarter_q)], allqc.at[k], cr1_s.at[0, j], cr1_r.at[0, k], {"rep": j})

    def x_rows(c, core):
        return cols(core * xparts + c, part_t // xparts)

    for c in range(xparts):
        for j in targets:
            block = allx.at[k, x_rows(c, t)]
            send(block, block, xr_s.at[c, 0, j], xr_r.at[c, 0, k], {"rep": j})

    for j in from_fs:
        block = allo.at[j, mine_po]
        arrived(block, po_s.at[j], po_r.at[j], {"fs": j})
        send(block, block, pt_s.at[0, j], pt_r.at[0, j], other)

    def pq_step(d):
        for has, j, on, to, way in sides(d):
            block = allq.at[j, mine_pq]
            arrived(block, pq_s.at[j, way], pq_r.at[j], {"fs": j}, has)
            send(block, block, pq_s.at[j, way], pq_r.at[j], {"fs": to}, on)
            send(block, block, pt_s.at[1, j], pt_r.at[1, j], other, has)

    if n > 1:
        pq_step(1)
    if across:
        for which, (source, to) in enumerate(((near, far), (far, near))):
            piece = alla.at[beyond, half_rows(part_t, which)]
            arrived(piece, ar_s.at[1 + which, beyond], ar_r.at[1 + which, beyond], {"rep": beyond})
            send(piece, piece, at_s.at[1 + which, beyond], at_r.at[1 + which, beyond], other)
        for source in targets:
            block = alla.at[source, cols(1 - t, part_t)]
            arrived(block, at_s.at[0, source], at_r.at[0, source], other)
        for which in range(2):
            piece = alla.at[beyond, cols(2 * (1 - t) + which, part_t // 2)]
            arrived(piece, at_s.at[1 + which, beyond], at_r.at[1 + which, beyond], other)
    else:
        for j in from_rep:
            block = alla.at[j, mine_t]
            arrived(block, ar_s.at[0, j], ar_r.at[0, j], {"rep": j})
            send(block, block, at_s.at[0, j], at_r.at[0, j], other)
        for j in from_rep:
            arrived(alla.at[j, cols(1 - t, part_t)], at_s.at[0, j], at_r.at[0, j], other)
    for j in from_fs:
        arrived(allo.at[j, their_po], pt_s.at[0, j], pt_r.at[0, j], other)
    for j in rep_peers:
        arrived(alloc.at[j], cr1_s.at[1, j], cr1_r.at[1, j], {"rep": j})
    load_oc_own.wait()

    def projected(load, factor, cot):
        load, factor, cot = (v[...].reshape(-1, v.shape[-1]) for v in (load, factor, cot))
        turned = jnp.dot(load, factor, preferred_element_type=F32).T
        high = turned.astype(BF16)
        rest = (turned - high.astype(F32)).astype(BF16)
        return jnp.dot(high, cot, preferred_element_type=F32) + jnp.dot(rest, cot, preferred_element_type=F32)

    sbo[...] = projected(alla, allo, alloc).reshape(n, low_rows, quarter_o)
    for j in fs_peers:
        send(sbo.at[j], r2o.at[f], r2_s.at[1, j], r2_r.at[1, f], {"fs": j})

    def x_step(c):
        for which, (source, to) in enumerate(((near, far), (far, near))):
            block = allx.at[source, x_rows(c, t)]
            arrived(block, xr_s.at[c, 0, source], xr_r.at[c, 0, source], {"rep": source})
            size = part_t // xparts
            piece = allx.at[source, cols(2 * (t * xparts + c) + which, size // 2)]
            send(piece, piece, xr_s.at[c, 1 + which, beyond], xr_r.at[c, 1 + which, source], {"rep": to})
            send(block, block, xt_s.at[c, 0, source], xt_r.at[c, 0, source], other)

    if n > 2:
        pq_step(2)
    if across:
        x_step(0)
    for d in range(3, n):
        pq_step(d)
    if across:
        for c in range(1, xparts):
            x_step(c)
        for c in range(xparts):
            for which in range(2):
                piece = allx.at[beyond, cols(2 * (t * xparts + c) + which, part_t // xparts // 2)]
                arrived(piece, xr_s.at[c, 1 + which, beyond], xr_r.at[c, 1 + which, beyond], {"rep": beyond})
                send(piece, piece, xt_s.at[c, 1 + which, beyond], xt_r.at[c, 1 + which, beyond], other)
        for c in range(xparts):
            for source in targets:
                arrived(allx.at[source, x_rows(c, 1 - t)], xt_s.at[c, 0, source], xt_r.at[c, 0, source], other)
            for which in range(2):
                piece = allx.at[beyond, cols(2 * ((1 - t) * xparts + c) + which, part_t // xparts // 2)]
                arrived(piece, xt_s.at[c, 1 + which, beyond], xt_r.at[c, 1 + which, beyond], other)
    else:
        for c in range(xparts):
            for j in from_rep:
                block = allx.at[j, x_rows(c, t)]
                arrived(block, xr_s.at[c, 0, j], xr_r.at[c, 0, j], {"rep": j})
                send(block, block, xt_s.at[c, 0, j], xt_r.at[c, 0, j], other)
        for c in range(xparts):
            for j in from_rep:
                arrived(allx.at[j, x_rows(c, 1 - t)], xt_s.at[c, 0, j], xt_r.at[c, 0, j], other)
    for j in from_fs:
        arrived(allq.at[j, their_pq], pt_s.at[1, j], pt_r.at[1, j], other)
    for j in rep_peers:
        arrived(allqc.at[j], cr1_s.at[0, j], cr1_r.at[0, j], {"rep": j})
    load_qc_own.wait()
    sbq[...] = projected(allx, allq, allqc).reshape(n, low_rows, quarter_q)
    for j in fs_peers:
        send(sbq.at[j], r2q.at[f], r2_s.at[0, j], r2_r.at[0, f], {"fs": j})

    def update(low_sum, first, second):
        first_new = beta_first * first + (1.0 - beta_first) * low_sum
        second_new = beta_second * second + (1.0 - beta_second) * low_sum * low_sum
        return first_new, second_new, first_new / (jnp.sqrt(second_new) + adam_eps)

    for copy in load_moments:
        copy.wait()
    kinds = (
        (quarter_q, sbq, r2q, lowgq, halfq, fqv, sqv, nfq, nsq),
        (quarter_o, sbo, r2o, lowgo, halfo, fov, sov, nfo, nso),
    )

    def reduced(i):
        width, own, got, gathered, half, first, second, new_first, new_second = kinds[i]
        low = own[f]
        for j in fs_peers:
            arrived(got.at[j], r2_s.at[i, j], r2_r.at[i, j], {"fs": j})
            low += got[j]
        gathered[k] = low

    def moments(i, m):
        width, own, got, gathered, half, first, second, new_first, new_second = kinds[i]
        at = cols(m, width)
        one, two, normed = update(gathered[m], first[:, at], second[:, at])
        new_first[:, at] = one
        new_second[:, at] = two
        half[m, f] = normed.astype(BF16)
        return normed

    def share(i):
        gathered, half = kinds[i][3], kinds[i][4]
        for j in fs_peers:
            send(half.at[k, f], half.at[k, f], hz_s.at[i, j], hz_r.at[i, f], {"fs": j})
        for m in rep_peers:
            send(gathered.at[k], gathered.at[k], lg_s.at[i, m], lg_r.at[i, k], {"rep": m})

    def squares(normed):
        return jnp.sum(normed * normed, axis=0, keepdims=True).reshape(1, -1, 128).sum(axis=1)

    reduced(1)
    square_o = squares(moments(1, k))
    share(1)
    reduced(0)
    square_q = squares(moments(0, k))
    tz[me] = square_q + square_o

    def tell(i, carry):
        remote(tz.at[me], tz.at[me], tz_s, tz_r, device(lax.rem(me + i, total))).start()
        return carry

    lax.fori_loop(1, total, tell, 0)
    share(0)

    def spread_half(i):
        half = kinds[i][4]
        for j in from_fs:
            arrived(half.at[k, j], hz_s.at[i, j], hz_r.at[i, j], {"fs": j})
            for m in rep_peers:
                send(half.at[k, j], half.at[k, j], hr_s.at[i, j, m], hr_r.at[i, j, k], {"rep": m})

    def gathered_moments(i):
        for m in from_rep:
            arrived(kinds[i][3].at[m], lg_s.at[i, m], lg_r.at[i, m], {"rep": m})
            moments(i, m)

    spread_half(1)
    gathered_moments(1)
    spread_half(0)
    for copy in load_weights:
        copy.wait()
    others = tz.at[pl.ds(0, total - 1)]
    remote(others, others, tz_s, tz_r, other).wait_recv()
    scale = lax.rsqrt(jnp.sum(jnp.sum(tz[...], axis=0), axis=-1, keepdims=True) / entries + mean_eps)

    outs = (
        (pq_step, quarter_q, halfq, wqv, nwq, stq, cpq, rows_q, allq),
        (None, quarter_o, halfo, wov, nwo, sto, cpo, rows_o, allo),
    )

    def weights(i, index):
        _, width, half, old, new, step, copy, rows, proj = outs[i]
        at = cols(index, width)
        block = half[index].reshape(rank, width)
        moved = scale * jnp.dot(proj[f], block, preferred_element_type=F32)
        fresh = old[:, at] - learn_rate * moved
        step[:, at] = moved
        new[:, at] = fresh
        copy[cols(f, rows), at] = fresh.astype(BF16)

    chunks = [(i, p) for p in range(parts) for i in range(2)]

    def block_of(c, j, m):
        i, p = chunks[c]
        copy, rows, width = outs[i][6], outs[i][7], outs[i][1]
        return copy.at[cols(j * parts + p, rows // parts), cols(m, width)]

    for i in range(2):
        weights(i, k)
        for c, (kind, p) in enumerate(chunks):
            if kind == i:
                block = block_of(c, f, k)
                for cond, to, way in outward:
                    send(block, block, cz_s.at[c, f, way], cz_r.at[c, f], {"fs": to}, cond)

    def relay(d):
        for c, (i, p) in enumerate(chunks):
            source, to = (near, far) if i == 0 else (far, near)
            for has, j, on, onward, way in sides(d):
                block = block_of(c, j, source)
                arrived(block, cr_s.at[c, j, source], cr_r.at[c, j, source], {"rep": source}, has)
                send(block, block, cr_s.at[c, j, beyond], cr_r.at[c, j, source], {"rep": to}, has)

    for d in range(1, n):
        for c in range(len(chunks)):
            for has, j, on, onward, way in sides(d):
                block = block_of(c, j, k)
                arrived(block, cz_s.at[c, j, way], cz_r.at[c, j], {"fs": j}, has)
                send(block, block, cz_s.at[c, j, way], cz_r.at[c, j], {"fs": onward}, on)
                for m in targets:
                    send(block, block, cr_s.at[c, j, m], cr_r.at[c, j, k], {"rep": m}, has)
        if d == 1:
            gathered_moments(0)
            for m in from_rep:
                for i in range(2):
                    for j in from_fs:
                        arrived(kinds[i][4].at[m, j], hr_s.at[i, j, m], hr_r.at[i, j, m], {"rep": m})
                    weights(i, m)
        if across and d > 1:
            relay(d - 1)
    if n == 1:
        gathered_moments(0)
        for m in from_rep:
            for i in range(2):
                weights(i, m)
    if across and n > 1:
        relay(n - 1)
    for j in from_fs:
        for c, (i, p) in enumerate(chunks):
            late = ([far, beyond] if i == 0 else [near, beyond]) if across else from_rep
            for m in late:
                arrived(block_of(c, j, m), cr_s.at[c, j, m], cr_r.at[c, j, m], {"rep": m})
    for cond, copy in sent:
        run(cond, copy.wait_send)
    remote(others, others, tz_s, tz_r, other).wait_send()


def place(pieces, *refs):
    count = len(pieces)
    sems = refs[-1]
    copies = []
    for i, many in enumerate(pieces):
        rows = refs[i].shape[0] // many
        for p in range(many):
            at = pl.ds(p * rows, rows)
            copies.append(pltpu.make_async_copy(refs[i].at[at], refs[count + i].at[at], sems.at[len(copies)]))
    for copy in copies:
        copy.start()
    for copy in copies:
        copy.wait()


def solution(mesh):
    n, r, tp = mesh.shape["fs"], mesh.shape["rep"], mesh.shape["tp"]

    def local(*args):
        x, qc, a, oc, pq, po, wq, wo, fq, sq, fo, so = args
        rank = pq.shape[1]
        low_rows = fq.shape[0]
        quarter_q, quarter_o = fq.shape[1] // r, fo.shape[1] // r
        entries = rank * (fq.shape[1] + fo.shape[1]) * tp
        parts = 2 if n <= 8 else 1
        xparts = 2
        total = n * r * tp
        shape = jax.ShapeDtypeStruct
        like = lambda v: shape(v.shape, v.dtype)
        vmem = lambda v: pltpu.VMEM(v.shape, v.dtype)
        dma = pltpu.SemaphoreType.DMA
        made = pl.pallas_call(
            functools.partial(kernel, n, r, tp, entries, parts, xparts),
            out_shape=(
                like(wq), like(wo), like(wq), like(wo), like(fq), like(sq), like(fo), like(so),
                shape((n * wq.shape[0], wq.shape[1]), BF16),
                shape((n * wo.shape[0], wo.shape[1]), BF16),
            ),
            in_specs=[pl.BlockSpec(memory_space=pl.ANY)] * 12,
            out_specs=[pl.BlockSpec(memory_space=pltpu.VMEM)] * 10,
            scratch_shapes=[
                pltpu.VMEM((n,) + pq.shape, BF16),
                pltpu.VMEM((n,) + po.shape, BF16),
                pltpu.VMEM((r,) + x.shape, BF16),
                pltpu.VMEM((r,) + a.shape, BF16),
                vmem(qc), vmem(oc),
                pltpu.VMEM((r, qc.shape[0], quarter_q), BF16),
                pltpu.VMEM((r, oc.shape[0], quarter_o), BF16),
                vmem(wq), vmem(wo), vmem(fq), vmem(sq), vmem(fo), vmem(so),
                pltpu.VMEM((n, low_rows, quarter_q), F32),
                pltpu.VMEM((n, low_rows, quarter_o), F32),
                pltpu.VMEM((n, low_rows, quarter_q), F32),
                pltpu.VMEM((n, low_rows, quarter_o), F32),
                pltpu.VMEM((r, low_rows, quarter_q), F32),
                pltpu.VMEM((r, low_rows, quarter_o), F32),
                pltpu.VMEM((r, n, low_rows, quarter_q), BF16),
                pltpu.VMEM((r, n, low_rows, quarter_o), BF16),
                pltpu.VMEM((total, 1, 128), F32),
                dma((14,)),
                dma((n,)), dma((n,)), dma((n, 2)), dma((n,)), dma((2, n)), dma((2, n)),
                dma((3, r)), dma((3, r)), dma((3, r)), dma((3, r)),
                dma((xparts, 3, r)), dma((xparts, 3, r)), dma((xparts, 3, r)), dma((xparts, 3, r)),
                dma((2, r)), dma((2, r)),
                dma((2, n)), dma((2, n)), dma((2, r)), dma((2, r)), dma((2, n)), dma((2, n)),
                dma((2, n, r)), dma((2, n, r)), dma(()), dma(()),
                dma((2 * parts, n, 2)), dma((2 * parts, n)), dma((2 * parts, n, r)), dma((2 * parts, n, r)),
            ],
            compiler_params=pltpu.CompilerParams(collective_id=0, has_side_effects=True),
        )(*args)
        pieces = tuple(max(1, min(8, v.size * v.dtype.itemsize // 2**18)) for v in made)
        return pl.pallas_call(
            functools.partial(place, pieces),
            out_shape=tuple(like(v) for v in made),
            in_specs=[pl.BlockSpec(memory_space=pltpu.VMEM)] * len(made),
            out_specs=[pl.BlockSpec(memory_space=pl.ANY)] * len(made),
            scratch_shapes=[dma((sum(pieces),))],
        )(*made)

    both, rows = P(("fs", "rep"), "tp"), P("fs", "tp")
    whole = P(("fs", "rep"), None)
    return jax.shard_map(
        local,
        mesh=mesh,
        in_specs=(whole, both, whole, both, P("fs", None), P("fs", None)) + (rows,) * 6,
        out_specs=(rows,) * 8 + (P(None, "tp"),) * 2,
        check_vma=False,
    )
```

time: 104 us -> 92 us (0.88)
  the two profiles are of different devices: /device:TPU:25 before, /device:TPU:0 now
where the time goes in v1:
time: 92 us; the launch traced here: 91.9 us
  Pallas kernels  91.2 us (99%)
    pallas_call x1, Pallas kernels, local(): pl.pallas_call(functools.partial(kernel, n, r, tp, entries, parts, xparts...  83.7 us
    pallas_call x1, Pallas kernels, local(): pl.pallas_call(functools.partial(place, pieces), out_shape=tuple((like(v)...  7.53 us

profile of v1, /device:TPU:0, one launch (start us, length us, event | category | flops | bytes accessed | tf_op | source)
XLA Modules:
  0.0 91.9 jit_solution(7982184415701282954)
XLA Ops:
  0.6 83.7 %shard_map.195 = (f32[512,512]{1,0:T(8,128)}, f32[256,1024]{1,0:T(8,128)}, f32[512,512]{1,0:T(8,128)}, f32[256,1024]{1,0:T(8,128)}, f32[64,512]{1,0:T(8,128)}, /...) custom-call(bf16[128,2048]{1,0:T(8,128)(2,1)} %x_h.1, ...), custom_call_target="tpu_custom_call" | custom-call | tf_op jit(solution)/shard_map/pallas_call | solution.py:429
  84.3 7.5 %shard_map.196 = (f32[512,512]{1,0:T(8,128)}, f32[256,1024]{1,0:T(8,128)}, f32[512,512]{1,0:T(8,128)}, f32[256,1024]{1,0:T(8,128)}, f32[64,512]{1,0:T(8,128)}, /...) custom-call(f32[512,512]{1,0:T(8,128)} %get-tuple-element.20.refs_0_, ...), custom_call_target="tpu_custom_call" | custom-call | tf_op jit(solution)/shard_map/pallas_call | solution.py:468

commit v2 on v1

--- a/solution.py
+++ b/solution.py
@@ -433,7 +433,7 @@
                 shape((n * wq.shape[0], wq.shape[1]), BF16),
                 shape((n * wo.shape[0], wo.shape[1]), BF16),
             ),
-            in_specs=[pl.BlockSpec(memory_space=pl.ANY)] * 12,
+            in_specs=[pl.BlockSpec(memory_space=pltpu.HBM)] * 12,
             out_specs=[pl.BlockSpec(memory_space=pltpu.VMEM)] * 10,
             scratch_shapes=[
                 pltpu.VMEM((n,) + pq.shape, BF16),
@@ -462,8 +462,8 @@
                 dma((2, n, r)), dma((2, n, r)), dma(()), dma(()),
                 dma((2 * parts, n, 2)), dma((2 * parts, n)), dma((2 * parts, n, r)), dma((2 * parts, n, r)),
             ],
-            compiler_params=pltpu.CompilerParams(collective_id=0, has_side_effects=True),
-        )(*args)
+            compiler_params=pltpu.CompilerParams(collective_id=0, has_side_effects=True, vmem_limit_bytes=24 * 2**20),
+        )(*(pltpu.with_memory_space_constraint(v, pltpu.HBM) for v in args))
         pieces = tuple(max(1, min(8, v.size * v.dtype.itemsize // 2**18)) for v in made)
         return pl.pallas_call(
             functools.partial(place, pieces),
@@ -471,6 +471,7 @@
             in_specs=[pl.BlockSpec(memory_space=pltpu.VMEM)] * len(made),
             out_specs=[pl.BlockSpec(memory_space=pl.ANY)] * len(made),
             scratch_shapes=[dma((sum(pieces),))],
+            compiler_params=pltpu.CompilerParams(vmem_limit_bytes=16 * 2**20),
         )(*made)
 
     both, rows = P(("fs", "rep"), "tp"), P("fs", "tp")

time: 92 us -> 84.9 us (0.923)
  Pallas kernels: 91.2 us -> 84.1 us
    pallas_call x1, Pallas kernels: 7.53 us -> 3.82 us  [local(): pl.pallas_call(functools.partial(place, pieces), out_shape=tuple((like(v)...]
    pallas_call x1, Pallas kernels: 83.7 us -> 80.2 us  [local(): pl.pallas_call(functools.partial(kernel, n, r, tp, entries, parts, xparts...]
where the time goes in v2:
time: 84.9 us; the launch traced here: 84.7 us
  Pallas kernels  84.1 us (99%)
    pallas_call x1, Pallas kernels, local(): pl.pallas_call(functools.partial(kernel, n, r, tp, entries, parts, xparts...  80.2 us
    pallas_call x1, Pallas kernels, local(): pl.pallas_call(functools.partial(place, pieces), out_shape=tuple((like(v)...  3.82 us

profile of v2, /device:TPU:0, one launch (start us, length us, event | category | flops | bytes accessed | tf_op | source)
XLA Modules:
  0.0 84.7 jit_solution(14208511037398873453)
XLA Ops:
  0.6 80.2 %shard_map.195 = (f32[512,512]{1,0:T(8,128)S(1)}, f32[256,1024]{1,0:T(8,128)S(1)}, f32[512,512]{1,0:T(8,128)S(1)}, f32[256,1024]{1,0:T(8,128)S(1)}, f32[64,512]{...) custom-call(bf16[128,2048]{1,0:T(8,128)(2,1)} %x_h.1, ...), custom_call_target="tpu_custom_call" | custom-call | tf_op jit(solution)/shard_map/pallas_call | solution.py:429
  80.9 3.8 %shard_map.196 = (f32[512,512]{1,0:T(8,128)}, f32[256,1024]{1,0:T(8,128)}, f32[512,512]{1,0:T(8,128)}, f32[256,1024]{1,0:T(8,128)}, f32[64,512]{1,0:T(8,128)}, /...) custom-call(f32[512,512]{1,0:T(8,128)S(1)} %get-tuple-element.20.ref, ...), custom_call_target="tpu_custom_call" | custom-call | tf_op jit(solution)/shard_map/pallas_call | solution.py:468

commit v3 on v2

v3 whole, which is shorter than its diff:
```python
import functools
import math

import jax
import jax.numpy as jnp
from jax import lax
from jax.experimental import pallas as pl
from jax.experimental.pallas import tpu as pltpu
from jax.sharding import PartitionSpec as P

beta_first = 0.9
beta_second = 0.95
adam_eps = 1e-08
mean_eps = 1e-06
learn_rate = 0.02

MESH = pl.DeviceIdType.MESH
F32 = jnp.float32
BF16 = jnp.bfloat16


def kernel(
    n, r, tp, entries, parts, xparts, qparts, ahead, extras,
    x_h, qc_h, a_h, oc_h, pq_h, po_h, wq_h, wo_h, fq_h, sq_h, fo_h, so_h,
    nwq, nwo, stq, sto, nfq, nsq, nfo, nso, cpq, cpo,
    allq, allo, allx, alla, qcv, ocv, allqc, alloc, wqv, wov, fqv, sqv, fov, sov,
    sbq, sbo, r2q, r2o, lowgq, lowgo, halfq, halfo, tz, early,
    ld, gone, line_s, po_r, pq_r, ar_r, xr_r, pt_r, at_r, xt_r, cr1_r, r2_r, lg_r, hz_r, hr_r,
    tz_s, tz_r, cz_r, cr_r, late_r, ex_r, we_r,
):
    f, k, t = lax.axis_index("fs"), lax.axis_index("rep"), lax.axis_index("tp")
    other = {"tp": 1 - t}
    total = n * r * tp
    me = (f * r + k) * tp + t
    rows_q, rank = pq_h.shape
    rows_o = po_h.shape[0]
    low_rows = fq_h.shape[0]
    tokens = x_h.shape[0]
    quarter_q, quarter_o = fq_h.shape[1] // r, fo_h.shape[1] // r
    fs_peers = [lax.rem(f + d, n) for d in range(1, n)]
    rep_peers = [lax.rem(k + d, r) for d in range(1, r)]
    from_fs, from_rep = fs_peers[::-1], rep_peers[::-1]
    across = r == 4
    if across:
        near, far = k + 1 - 2 * lax.rem(k, 2), lax.rem(k + 2, r)
        beyond = lax.rem(near + 2, r)
        targets = [near, far]
    else:
        targets = rep_peers

    def device(p):
        return {"fs": lax.div(p, r * tp), "rep": lax.rem(lax.div(p, tp), r), "tp": lax.rem(p, tp)}

    def remote(src, dst, ssem, rsem, where):
        return pltpu.make_async_remote_copy(
            src_ref=src, dst_ref=dst, send_sem=ssem, recv_sem=rsem, device_id=where, device_id_type=MESH
        )

    def run(cond, action):
        if cond is None:
            action()
        else:
            pl.when(cond)(action)

    row_bytes = cpq.shape[1] * 2
    limit = cpq.shape[0] * row_bytes
    bulk = [0, 0, 0, 0]

    def size_of(ref):
        return math.prod(ref.shape) * jnp.dtype(ref.dtype).itemsize

    def send(src, dst, rsem, where, cond=None, counted=True, group=None):
        if group is None:
            if bulk[-1] + size_of(src) > limit:
                bulk.append(0)
            group = len(bulk) - 1
        if counted:
            bulk[group] += size_of(src)
        run(cond, remote(src, dst, gone.at[group], rsem, where).start)

    lined = {0: 0, 1: 0}

    def send_line(group, src, dst, rsem, where, cond, own=False):
        if own:
            lined[group] += size_of(src)
        run(cond, remote(src, dst, line_s.at[group], rsem, where).start)

    def arrived(dst, rsem, where, cond=None):
        run(cond, remote(dst, dst, gone.at[0], rsem, where).wait_recv)

    def drain(count, sem, out, cond=None):
        whole, small = count // (8 * row_bytes), count % (8 * row_bytes) // (8 * 128 * 2)
        refs = [cpq.at[pl.ds(0, 8 * whole)]] if whole else []
        refs += [cpq.at[pl.ds(0, 8), pl.ds(0, 128 * small)]] if small else []
        for ref in refs:
            copy = remote(ref, ref, sem, sem, other)
            run(cond, copy.wait_send if out else copy.wait_recv)

    def cols(index, width):
        return pl.ds(pl.multiple_of(index * width, width), width)

    barrier = pltpu.get_barrier_semaphore()

    def everyone(action):
        if total > 32:
            def step(i, carry):
                action(device(lax.rem(me + i, total)))
                return carry

            lax.fori_loop(1, total, step, 0)
            return
        fs = [lax.rem(f + d, n) for d in range(n)]
        rep = [lax.rem(k + d, r) for d in range(r)]
        for a in reversed(range(n)):
            for b in reversed(range(r)):
                for c in range(tp):
                    if a or b or c:
                        action({"fs": fs[a], "rep": rep[b], "tp": 1 - t if c else t})

    everyone(lambda where: pl.semaphore_signal(barrier, inc=1, device_id=where, device_id_type=MESH))

    loads = []

    def load(src, dst):
        copy = pltpu.make_async_copy(src, dst, ld.at[len(loads)])
        copy.start()
        loads.append(copy)
        return copy

    load_po = load(po_h, allo.at[f])
    load_a = load(a_h, alla.at[0])
    load_oc = load(oc_h, ocv)
    load_pq = load(pq_h, allq.at[f])
    load_qc = load(qc_h, qcv)
    load_x = load(x_h, allx.at[0])
    load_oc_own = load(oc_h.at[:, cols(k, quarter_o)], alloc.at[0])
    load_qc_own = load(qc_h.at[:, cols(k, quarter_q)], allqc.at[0])
    load_moments = [load(s, d) for s, d in ((fo_h, fov), (so_h, sov), (fq_h, fqv), (sq_h, sqv))]
    load_weights = [load(s, d) for s, d in ((wq_h, wqv), (wo_h, wov))]

    load_po.wait()
    load_a.wait()
    load_oc.wait()
    pl.semaphore_wait(barrier, total - 1)

    def sides(d):
        return (
            (f >= d, lax.rem(f + n - d, n), jnp.logical_and(f >= d, f < n - 1), lax.rem(f + 1, n), 0),
            (f + d < n, lax.rem(f + d, n), jnp.logical_and(f + d < n, f > 0), lax.rem(f + n - 1, n), 1),
        )

    outward = ((f < n - 1, lax.rem(f + 1, n), 0), (f > 0, lax.rem(f + n - 1, n), 1))

    part_po, part_pq, part_t = rows_o // tp, rows_q // tp, tokens // tp
    mine_po, mine_t = cols(t, part_po), cols(t, part_t)
    piece_pq, piece_x = part_pq // qparts, part_t // xparts

    def pq_rows(c, core):
        return cols(core * qparts + c, piece_pq)

    def x_rows(c, core):
        return cols(core * xparts + c, piece_x)

    if across:
        slots = [(near, 1), (far, 2)]
        rep_slots = slots + [(beyond, 3)]
        turns = ((near, 1, far), (far, 2, near))
        deposit = {1: 1, 2: 2, 3: 3}
    else:
        rep_slots = slots = [(j, d) for d, j in enumerate(rep_peers, 1)]
        deposit = {d: r - d for d in range(1, r)}

    def post(whole, rows, sems, at, peers):
        for j, d in peers:
            send(whole.at[0, rows], whole.at[deposit[d], rows], sems.at[at + (deposit[d] - 1,)], {"rep": j})

    def pass_on(whole, rows_of, sems, over, at):
        for which, (source, d, to) in enumerate(turns):
            block = whole.at[d, rows_of(t)]
            arrived(block, sems.at[at + (d - 1,)], {"rep": source})
            rows = rows_of(t, which)
            send(whole.at[d, rows], whole.at[3, rows], sems.at[at + (2 + which,)], {"rep": to})
            send(block, block, over.at[0], other)

    def last_pieces(whole, rows_of, sems, over, at):
        for which in range(2):
            block = whole.at[3, rows_of(t, which)]
            arrived(block, sems.at[at + (2 + which,)], {"rep": beyond})
            send(block, block, over.at[1], other)

    def plain(whole, rows_of, sems, over, at):
        for j, d in slots:
            block = whole.at[d, rows_of(t)]
            arrived(block, sems.at[at + (d - 1,)], {"rep": j})
            send(block, block, over.at[0], other)

    def from_other(whole, over, last):
        if not last:
            arrived(whole.at[pl.ds(1, len(slots)), pl.ds(0, part_t)], over.at[0], other)
        elif across:
            arrived(whole.at[3, pl.ds(0, part_t)], over.at[1], other)

    def a_rows(core, which=None):
        return cols(core, part_t) if which is None else cols(2 * core + which, part_t // 2)

    def x_of(c):
        def rows_of(core, which=None):
            if which is None:
                return cols(core * xparts + c, piece_x)
            return cols(2 * (core * xparts + c) + which, piece_x // 2)

        return rows_of

    a_args = (alla, a_rows, ar_r, at_r, (0,))
    x_args = [(allx, x_of(c), xr_r, xt_r, (c,)) for c in range(xparts)]

    for j in fs_peers:
        block = allo.at[f, mine_po]
        send(block, block, po_r.at[f], {"fs": j})
    post(alla, mine_t, ar_r, (0,), slots)
    for j, d in rep_slots:
        send(ocv.at[:, cols(j, quarter_o)], alloc.at[deposit[d]], cr1_r.at[1], {"rep": j})
    load_pq.wait()
    for c in range(qparts):
        for cond, to, way in outward:
            block = allq.at[f, pq_rows(c, t)]
            send_line(0, block, block, pq_r.at[c, f], {"fs": to}, cond, way == 0)

    if across:
        pass_on(*a_args)
    load_qc.wait()
    load_x.wait()
    for j, d in rep_slots:
        send(qcv.at[:, cols(j, quarter_q)], allqc.at[deposit[d]], cr1_r.at[0], {"rep": j})
    for c in range(xparts):
        post(allx, x_rows(c, t), xr_r, (c,), slots)

    for j in from_fs:
        block = allo.at[j, mine_po]
        arrived(block, po_r.at[j], {"fs": j})
        send(block, block, pt_r.at[1], other)

    def pq_step(d, c):
        for has, j, on, to, way in sides(d):
            block = allq.at[j, pq_rows(c, t)]
            arrived(block, pq_r.at[c, j], {"fs": j}, has)
            send_line(0, block, block, pq_r.at[c, j], {"fs": to}, on)
            send(block, block, pt_r.at[0], other, has, way == 0, 0)

    if n > 1:
        pq_step(1, 0)
    if across:
        last_pieces(*a_args)
    else:
        plain(*a_args)
    for c in range(1, qparts):
        if n > 1:
            pq_step(1, c)
    for last in range(2):
        from_other(alla, at_r, last)
    if n > 1:
        arrived(allo.at[pl.ds(0, n - 1), pl.ds(0, part_po)], pt_r.at[1], other)
    arrived(alloc.at[pl.ds(1, r - 1)], cr1_r.at[1], other)
    load_oc_own.wait()

    def projected(load, factor, cot):
        load, factor, cot = (v.reshape(-1, v.shape[-1]) for v in (load, factor, cot))
        turned = jnp.dot(load, factor, preferred_element_type=F32).T
        high = turned.astype(BF16)
        rest = (turned - high.astype(F32)).astype(BF16)
        return jnp.dot(high, cot, preferred_element_type=F32) + jnp.dot(rest, cot, preferred_element_type=F32)

    sbo[...] = projected(alla[...], allo[...], alloc[...]).reshape(n, low_rows, quarter_o)

    if n > 2:
        for c in range(qparts):
            pq_step(2, c)
    if across:
        pass_on(*x_args[0])
    if across:
        for c in range(1, xparts):
            pass_on(*x_args[c])
    for j in fs_peers:
        send(sbo.at[j], r2o.at[f], r2_r.at[1], {"fs": j})
    for d in range(3, n):
        for c in range(qparts):
            pq_step(d, c)
    if across:
        for c in range(xparts - 1):
            last_pieces(*x_args[c])
    else:
        for c in range(xparts):
            plain(*x_args[c])
    from_other(allx, xt_r, 0)
    if n > 1:
        arrived(allq.at[pl.ds(0, n - 1), pl.ds(0, part_pq)], pt_r.at[0], other)
    arrived(allqc.at[pl.ds(1, r - 1)], cr1_r.at[0], other)
    load_qc_own.wait()
    if across:
        sbq[...] = projected(allx[:3], allq[...], allqc[:3]).reshape(n, low_rows, quarter_q)
        last_pieces(*x_args[xparts - 1])
        from_other(allx, xt_r, 1)
        sbq[...] += projected(allx[3], allq[...], allqc[3]).reshape(n, low_rows, quarter_q)
    else:
        sbq[...] = projected(allx[...], allq[...], allqc[...]).reshape(n, low_rows, quarter_q)
    for j in fs_peers:
        send(sbq.at[j], r2q.at[f], r2_r.at[0], {"fs": j})

    def update(low_sum, first, second):
        first_new = beta_first * first + (1.0 - beta_first) * low_sum
        second_new = beta_second * second + (1.0 - beta_second) * low_sum * low_sum
        return first_new, second_new, first_new / (jnp.sqrt(second_new) + adam_eps)

    for copy in load_moments:
        copy.wait()
    kinds = (
        (quarter_q, sbq, r2q, lowgq, halfq, fqv, sqv, nfq, nsq),
        (quarter_o, sbo, r2o, lowgo, halfo, fov, sov, nfo, nso),
    )

    def reduced(i):
        width, own, got, gathered, half, first, second, new_first, new_second = kinds[i]
        if n > 1:
            arrived(got.at[pl.ds(0, n - 1)], r2_r.at[i], other)
        low = own[f]
        for j in fs_peers:
            low += got[j]
        gathered[k] = low

    def moments(i, m):
        width, own, got, gathered, half, first, second, new_first, new_second = kinds[i]
        at = cols(m, width)
        one, two, normed = update(gathered[m], first[:, at], second[:, at])
        new_first[:, at] = one
        new_second[:, at] = two
        half[m, f] = normed.astype(BF16)
        return normed

    def share(i):
        gathered, half = kinds[i][3], kinds[i][4]
        for j in fs_peers:
            send(half.at[k, f], half.at[k, f], hz_r.at[i], {"fs": j})
        for m in rep_peers:
            send(gathered.at[k], gathered.at[k], lg_r.at[i], {"rep": m})

    def squares(normed):
        return jnp.sum(normed * normed, axis=0, keepdims=True).reshape(1, -1, 128).sum(axis=1)

    reduced(1)
    square_o = squares(moments(1, k))
    share(1)
    reduced(0)
    square_q = squares(moments(0, k))
    tz[me] = square_q + square_o

    everyone(lambda where: remote(tz.at[me], tz.at[me], tz_s, tz_r, where).start())
    share(0)

    def spread_half(i):
        half = kinds[i][4]
        if n > 1:
            arrived(half.at[k, pl.ds(0, n - 1)], hz_r.at[i], other)
        for m in rep_peers:
            for j in from_fs:
                send(half.at[k, j], half.at[k, j], hr_r.at[i, k], {"rep": m})

    def gathered_moments(i):
        if r > 1:
            arrived(kinds[i][3].at[pl.ds(0, r - 1)], lg_r.at[i], other)
        for m in from_rep:
            moments(i, m)

    early_rows = rows_q // parts
    first = pl.ds(0, early_rows)
    if ahead:
        for copy in load_weights:
            copy.wait()
        for j in fs_peers:
            send(wqv.at[first, cols(k, quarter_q)], early.at[f], we_r, {"fs": j})
    spread_half(1)
    gathered_moments(1)
    spread_half(0)
    if not ahead:
        for copy in load_weights:
            copy.wait()
    others = tz.at[pl.ds(0, total - 1)]
    remote(others, others, tz_s, tz_r, other).wait_recv()
    scale = lax.rsqrt(jnp.sum(jnp.sum(tz[...], axis=0), axis=-1, keepdims=True) / entries + mean_eps)

    outs = (
        (None, quarter_q, halfq, wqv, nwq, stq, cpq, rows_q, allq),
        (None, quarter_o, halfo, wov, nwo, sto, cpo, rows_o, allo),
    )

    def weights(i, index):
        _, width, half, old, new, step, copy, rows, proj = outs[i]
        at = cols(index, width)
        block = half[index].reshape(rank, width)
        moved = scale * jnp.dot(proj[f], block, preferred_element_type=F32)
        fresh = old[:, at] - learn_rate * moved
        step[:, at] = moved
        new[:, at] = fresh
        copy[cols(f, rows), at] = fresh.astype(BF16)

    chunks = [(i, p) for p in range(parts) for i in range(2)]
    along_fs = [0] * len(chunks)
    if across and ahead:
        for at, c in enumerate(extras, 1):
            along_fs[c] = at

    def block_of(c, j, m):
        i, p = chunks[c]
        copy, rows, width = outs[i][6], outs[i][7], outs[i][1]
        return copy.at[cols(j * parts + p, rows // parts), cols(m, width)]

    def spread(c, j, has=None, counted=True):
        i = chunks[c][0]
        block = block_of(c, j, k)
        for m in targets:
            final = not across or (m is near) == (i == 1)
            send(block, block, late_r if final else cr_r.at[c, j], {"rep": m}, has, counted, 1)

    for i in range(2):
        weights(i, k)
        for c, (kind, p) in enumerate(chunks):
            if kind == i and not (ahead and c == 0):
                block = block_of(c, f, k)
                for cond, to, way in outward:
                    send_line(1, block, block, cz_r.at[c, f], {"fs": to}, cond, way == 0)
    if ahead:
        arrived(early.at[pl.ds(0, n - 1)], we_r, other)
        block = halfq[k].reshape(rank, quarter_q)
        for j in from_fs:
            moved = scale * jnp.dot(allq[j, first], block, preferred_element_type=F32)
            cpq[cols(j * parts, early_rows), cols(k, quarter_q)] = (early[j] - learn_rate * moved).astype(BF16)
            spread(0, j)

    def relay(d):
        for c, (i, p) in enumerate(chunks):
            source, to = (near, far) if i == 0 else (far, near)
            for has, j, on, onward, way in sides(d):
                block = block_of(c, j, source)
                arrived(block, cr_r.at[c, j], {"rep": source}, has)
                if not along_fs[c]:
                    send(block, block, late_r, {"rep": to}, has, way == 0, 2)

    def extra(d):
        for c in range(len(chunks)):
            if along_fs[c]:
                for has, j, on, onward, way in sides(d):
                    block = block_of(c, j, beyond)
                    at = along_fs[c] - 1
                    arrived(block, ex_r.at[at, j], {"fs": j}, has)
                    send_line(0, block, block, ex_r.at[at, j], {"fs": onward}, on)

    def rest_of_weights():
        gathered_moments(0)
        for m in [beyond, near, far] if across else from_rep:
            for i in range(2):
                if n > 1:
                    arrived(kinds[i][4].at[m, pl.ds(0, n - 1)], hr_r.at[i, m], other)
                weights(i, m)
            if across and m is beyond:
                for c in range(len(chunks)):
                    if along_fs[c]:
                        block = block_of(c, f, beyond)
                        for cond, to, way in outward:
                            send_line(0, block, block, ex_r.at[along_fs[c] - 1, f], {"fs": to}, cond, way == 0)

    for d in range(1, n):
        for c in range(len(chunks)):
            if ahead and c == 0:
                continue
            for has, j, on, onward, way in sides(d):
                block = block_of(c, j, k)
                arrived(block, cz_r.at[c, j], {"fs": j}, has)
                send_line(1, block, block, cz_r.at[c, j], {"fs": onward}, on)
                spread(c, j, has, way == 0)
        if d == 1:
            rest_of_weights()
        if across and d > 1:
            relay(d - 1)
            extra(d - 1)
    if n == 1:
        rest_of_weights()
    if across and n > 1:
        relay(n - 1)
        extra(n - 1)
    if n > 1:
        count = 0
        for c in range(len(chunks)):
            times = r - 1 if not across else 1 if along_fs[c] else 2
            count += (n - 1) * times * size_of(block_of(c, f, k))
        drain(count, late_r, False)
    for g, count in enumerate(bulk):
        assert count <= limit
        drain(count, gone.at[g], True)
    for v in range(n):
        times = (v + 1 if v < n - 1 else 0) + (n - v if v > 0 else 0)
        for g in range(2):
            if times and lined[g]:
                drain(times * lined[g], line_s.at[g], True, f == v)
    remote(others, others, tz_s, tz_r, other).wait_send()


def place(pieces, *refs):
    count = len(pieces)
    sems = refs[-1]
    copies = []
    for i, many in enumerate(pieces):
        rows = refs[i].shape[0] // many
        for p in range(many):
            at = pl.ds(p * rows, rows)
            copies.append(pltpu.make_async_copy(refs[i].at[at], refs[count + i].at[at], sems.at[len(copies)]))
    for copy in copies:
        copy.start()
    for copy in copies:
        copy.wait()


def solution(mesh):
    n, r, tp = mesh.shape["fs"], mesh.shape["rep"], mesh.shape["tp"]

    def local(*args):
        x, qc, a, oc, pq, po, wq, wo, fq, sq, fo, so = args
        rank = pq.shape[1]
        low_rows = fq.shape[0]
        quarter_q, quarter_o = fq.shape[1] // r, fo.shape[1] // r
        entries = rank * (fq.shape[1] + fo.shape[1]) * tp
        parts = 4 if n <= 8 else 1
        xparts = qparts = 2
        ahead = r == 4 and parts == 4 and n > 1
        extras = (5, 6, 7)
        total = n * r * tp
        shape = jax.ShapeDtypeStruct
        like = lambda v: shape(v.shape, v.dtype)
        vmem = lambda v: pltpu.VMEM(v.shape, v.dtype)
        dma = pltpu.SemaphoreType.DMA
        made = pl.pallas_call(
            functools.partial(kernel, n, r, tp, entries, parts, xparts, qparts, ahead, extras),
            out_shape=(
                like(wq), like(wo), like(wq), like(wo), like(fq), like(sq), like(fo), like(so),
                shape((n * wq.shape[0], wq.shape[1]), BF16),
                shape((n * wo.shape[0], wo.shape[1]), BF16),
            ),
            in_specs=[pl.BlockSpec(memory_space=pltpu.HBM)] * 12,
            out_specs=[pl.BlockSpec(memory_space=pltpu.VMEM)] * 10,
            scratch_shapes=[
                pltpu.VMEM((n,) + pq.shape, BF16),
                pltpu.VMEM((n,) + po.shape, BF16),
                pltpu.VMEM((r,) + x.shape, BF16),
                pltpu.VMEM((r,) + a.shape, BF16),
                vmem(qc), vmem(oc),
                pltpu.VMEM((r, qc.shape[0], quarter_q), BF16),
                pltpu.VMEM((r, oc.shape[0], quarter_o), BF16),
                vmem(wq), vmem(wo), vmem(fq), vmem(sq), vmem(fo), vmem(so),
                pltpu.VMEM((n, low_rows, quarter_q), F32),
                pltpu.VMEM((n, low_rows, quarter_o), F32),
                pltpu.VMEM((n, low_rows, quarter_q), F32),
                pltpu.VMEM((n, low_rows, quarter_o), F32),
                pltpu.VMEM((r, low_rows, quarter_q), F32),
                pltpu.VMEM((r, low_rows, quarter_o), F32),
                pltpu.VMEM((r, n, low_rows, quarter_q), BF16),
                pltpu.VMEM((r, n, low_rows, quarter_o), BF16),
                pltpu.VMEM((total, 1, 128), F32),
                pltpu.VMEM((n, wq.shape[0] // parts, quarter_q) if ahead else (8, 128), F32),
                dma((14,)), dma((8,)), dma((2,)),
                dma((n,)), dma((qparts, n)), dma((1, max(r, 4))), dma((xparts, max(r, 4))),
                dma((2,)), dma((2,)), dma((2,)), dma((2,)), dma((2,)), dma((2,)), dma((2,)), dma((2, r)),
                dma(()), dma(()), dma((2 * parts, n)), dma((2 * parts, n)), dma(()), dma((len(extras), n)), dma(()),
            ],
            compiler_params=pltpu.CompilerParams(collective_id=0, has_side_effects=True, vmem_limit_bytes=24 * 2**20),
        )(*(pltpu.with_memory_space_constraint(v, pltpu.HBM) for v in args))
        pieces = tuple(max(1, min(8, v.size * v.dtype.itemsize // 2**18)) for v in made)
        return pl.pallas_call(
            functools.partial(place, pieces),
            out_shape=tuple(like(v) for v in made),
            in_specs=[pl.BlockSpec(memory_space=pltpu.VMEM)] * len(made),
            out_specs=[pl.BlockSpec(memory_space=pl.ANY)] * len(made),
            scratch_shapes=[dma((sum(pieces),))],
            compiler_params=pltpu.CompilerParams(vmem_limit_bytes=16 * 2**20),
        )(*made)

    both, rows = P(("fs", "rep"), "tp"), P("fs", "tp")
    whole = P(("fs", "rep"), None)
    return jax.shard_map(
        local,
        mesh=mesh,
        in_specs=(whole, both, whole, both, P("fs", None), P("fs", None)) + (rows,) * 6,
        out_specs=(rows,) * 8 + (P(None, "tp"),) * 2,
        check_vma=False,
    )
```

time: 84.9 us -> 72.8 us (0.86)
  Pallas kernels: 84.1 us -> 71.9 us
    pallas_call x1, Pallas kernels: 80.2 us -> 68.1 us  [local(): pl.pallas_call(functools.partial(kernel, n, r, tp, entries, parts, xparts...]
where the time goes in v3:
time: 72.8 us; the launch traced here: 72.6 us
  Pallas kernels  71.9 us (99%)
    pallas_call x1, Pallas kernels, local(): pl.pallas_call(functools.partial(kernel, n, r, tp, entries, parts, xparts...  68.1 us
    pallas_call x1, Pallas kernels, local(): pl.pallas_call(functools.partial(place, pieces), out_shape=tuple((like(v)...  3.82 us

profile of v3, /device:TPU:0, one launch (start us, length us, event | category | flops | bytes accessed | tf_op | source)
XLA Modules:
  0.0 72.6 jit_solution(13617654312757862867)
XLA Ops:
  0.6 68.1 %shard_map.195 = (f32[512,512]{1,0:T(8,128)S(1)}, f32[256,1024]{1,0:T(8,128)S(1)}, f32[512,512]{1,0:T(8,128)S(1)}, f32[256,1024]{1,0:T(8,128)S(1)}, f32[64,512]{...) custom-call(bf16[128,2048]{1,0:T(8,128)(2,1)} %x_h.1, ...), custom_call_target="tpu_custom_call" | custom-call | tf_op jit(solution)/shard_map/pallas_call | solution.py:539
  68.8 3.8 %shard_map.196 = (f32[512,512]{1,0:T(8,128)}, f32[256,1024]{1,0:T(8,128)}, f32[512,512]{1,0:T(8,128)}, f32[256,1024]{1,0:T(8,128)}, f32[64,512]{1,0:T(8,128)}, /...) custom-call(f32[512,512]{1,0:T(8,128)S(1)} %get-tuple-element.20.ref, ...), custom_call_target="tpu_custom_call" | custom-call | tf_op jit(solution)/shard_map/pallas_call | solution.py:575

commit v4 on v3

--- a/solution.py
+++ b/solution.py
@@ -20,7 +20,7 @@
 
 
 def kernel(
-    n, r, tp, entries, parts, xparts, qparts, ahead, extras,
+    n, r, tp, entries, layout, units, xparts, qparts, ahead,
     x_h, qc_h, a_h, oc_h, pq_h, po_h, wq_h, wo_h, fq_h, sq_h, fo_h, so_h,
     nwq, nwo, stq, sto, nfq, nsq, nfo, nso, cpq, cpo,
     allq, allo, allx, alla, qcv, ocv, allqc, alloc, wqv, wov, fqv, sqv, fov, sov,
@@ -34,10 +34,15 @@
     me = (f * r + k) * tp + t
     rows_q, rank = pq_h.shape
     rows_o = po_h.shape[0]
+    unit_q, unit_o = rows_q // units, rows_o // units
     low_rows = fq_h.shape[0]
     tokens = x_h.shape[0]
     quarter_q, quarter_o = fq_h.shape[1] // r, fo_h.shape[1] // r
-    fs_peers = [lax.rem(f + d, n) for d in range(1, n)]
+    if n == 4:
+        over = lax.rem(f + 2, n)
+        fs_peers = [over, over + 1 - 2 * lax.rem(over, 2), f + 1 - 2 * lax.rem(f, 2)]
+    else:
+        fs_peers = [lax.rem(f + d, n) for d in range(1, n)]
     rep_peers = [lax.rem(k + d, r) for d in range(1, r)]
     from_fs, from_rep = fs_peers[::-1], rep_peers[::-1]
     across = r == 4
@@ -214,18 +219,38 @@
     a_args = (alla, a_rows, ar_r, at_r, (0,))
     x_args = [(allx, x_of(c), xr_r, xt_r, (c,)) for c in range(xparts)]
 
-    for j in fs_peers:
+    for cond, to, way in outward:
         block = allo.at[f, mine_po]
-        send(block, block, po_r.at[f], {"fs": j})
+        send_line(0, block, block, po_r.at[f], {"fs": to}, cond, way == 0)
     post(alla, mine_t, ar_r, (0,), slots)
     for j, d in rep_slots:
         send(ocv.at[:, cols(j, quarter_o)], alloc.at[deposit[d]], cr1_r.at[1], {"rep": j})
     load_pq.wait()
-    for c in range(qparts):
+
+    def pq_out(c):
         for cond, to, way in outward:
             block = allq.at[f, pq_rows(c, t)]
             send_line(0, block, block, pq_r.at[c, f], {"fs": to}, cond, way == 0)
 
+    def pq_step(d, c):
+        for has, j, on, to, way in sides(d):
+            block = allq.at[j, pq_rows(c, t)]
+            arrived(block, pq_r.at[c, j], {"fs": j}, has)
+            send_line(0, block, block, pq_r.at[c, j], {"fs": to}, on)
+            send(block, block, pt_r.at[0], other, has, way == 0, 0)
+
+    def po_step(d):
+        for has, j, on, to, way in sides(d):
+            block = allo.at[j, mine_po]
+            arrived(block, po_r.at[j], {"fs": j}, has)
+            send_line(0, block, block, po_r.at[j], {"fs": to}, on)
+            send(block, block, pt_r.at[1], other, has, way == 0, 3)
+
+    pq_out(0)
+    if n > 1:
+        po_step(1)
+    for c in range(1, qparts):
+        pq_out(c)
     if across:
         pass_on(*a_args)
     load_qc.wait()
@@ -234,28 +259,21 @@
         send(qcv.at[:, cols(j, quarter_q)], allqc.at[deposit[d]], cr1_r.at[0], {"rep": j})
     for c in range(xparts):
         post(allx, x_rows(c, t), xr_r, (c,), slots)
-
-    for j in from_fs:
-        block = allo.at[j, mine_po]
-        arrived(block, po_r.at[j], {"fs": j})
-        send(block, block, pt_r.at[1], other)
-
-    def pq_step(d, c):
-        for has, j, on, to, way in sides(d):
-            block = allq.at[j, pq_rows(c, t)]
-            arrived(block, pq_r.at[c, j], {"fs": j}, has)
-            send_line(0, block, block, pq_r.at[c, j], {"fs": to}, on)
-            send(block, block, pt_r.at[0], other, has, way == 0, 0)
-
     if n > 1:
         pq_step(1, 0)
+    if n > 2:
+        po_step(2)
+    for c in range(1, qparts):
+        if n > 1:
+            pq_step(1, c)
     if across:
         last_pieces(*a_args)
     else:
         plain(*a_args)
-    for c in range(1, qparts):
-        if n > 1:
-            pq_step(1, c)
+    if n > 2:
+        pq_step(2, 0)
+    for d in range(3, n):
+        po_step(d)
     for last in range(2):
         from_other(alla, at_r, last)
     if n > 1:
@@ -272,16 +290,30 @@
 
     sbo[...] = projected(alla[...], allo[...], alloc[...]).reshape(n, low_rows, quarter_o)
 
+    def w_step(d):
+        for has, j, on, to, way in sides(d):
+            block = early.at[j]
+            arrived(block, we_r.at[j], {"fs": j}, has)
+            send_line(1, block, block, we_r.at[j], {"fs": to}, on)
+
+    early_rows = unit_q * layout[0][1]
+    first = pl.ds(0, early_rows)
     if n > 2:
-        for c in range(qparts):
+        for c in range(1, qparts):
             pq_step(2, c)
     if across:
         pass_on(*x_args[0])
+    if ahead:
+        for copy in load_weights:
+            copy.wait()
+        block = wqv.at[first, cols(k, quarter_q)]
+        for cond, to, way in outward:
+            send_line(1, block, early.at[f], we_r.at[f], {"fs": to}, cond, way == 0)
+    for j in fs_peers:
+        send(sbo.at[j], r2o.at[f], r2_r.at[1], {"fs": j})
     if across:
         for c in range(1, xparts):
             pass_on(*x_args[c])
-    for j in fs_peers:
-        send(sbo.at[j], r2o.at[f], r2_r.at[1], {"fs": j})
     for d in range(3, n):
         for c in range(qparts):
             pq_step(d, c)
@@ -298,6 +330,8 @@
     load_qc_own.wait()
     if across:
         sbq[...] = projected(allx[:3], allq[...], allqc[:3]).reshape(n, low_rows, quarter_q)
+        if ahead:
+            w_step(1)
         last_pieces(*x_args[xparts - 1])
         from_other(allx, xt_r, 1)
         sbq[...] += projected(allx[3], allq[...], allqc[3]).reshape(n, low_rows, quarter_q)
@@ -340,49 +374,70 @@
         gathered, half = kinds[i][3], kinds[i][4]
         for j in fs_peers:
             send(half.at[k, f], half.at[k, f], hz_r.at[i], {"fs": j})
-        for m in rep_peers:
-            send(gathered.at[k], gathered.at[k], lg_r.at[i], {"rep": m})
-
-    def squares(normed):
-        return jnp.sum(normed * normed, axis=0, keepdims=True).reshape(1, -1, 128).sum(axis=1)
-
-    reduced(1)
-    square_o = squares(moments(1, k))
-    share(1)
-    reduced(0)
-    square_q = squares(moments(0, k))
-    tz[me] = square_q + square_o
-
-    everyone(lambda where: remote(tz.at[me], tz.at[me], tz_s, tz_r, where).start())
-    share(0)
+        for m in targets:
+            send(gathered.at[k], gathered.at[k], lg_r.at[i, k], {"rep": m})
 
     def spread_half(i):
         half = kinds[i][4]
         if n > 1:
             arrived(half.at[k, pl.ds(0, n - 1)], hz_r.at[i], other)
-        for m in rep_peers:
+        for m in targets:
             for j in from_fs:
                 send(half.at[k, j], half.at[k, j], hr_r.at[i, k], {"rep": m})
 
-    def gathered_moments(i):
-        if r > 1:
-            arrived(kinds[i][3].at[pl.ds(0, r - 1)], lg_r.at[i], other)
-        for m in from_rep:
+    def way_of(i):
+        return (near, far) if i == 0 else (far, near)
+
+    def lows_in(i, peers):
+        for m in peers:
+            arrived(kinds[i][3].at[m], lg_r.at[i, m], {"rep": m})
             moments(i, m)
 
-    early_rows = rows_q // parts
-    first = pl.ds(0, early_rows)
+    def low_on(i):
+        source, to = way_of(i)
+        block = kinds[i][3].at[source]
+        arrived(block, lg_r.at[i, source], {"rep": source})
+        send(block, block, lg_r.at[i, source], {"rep": to})
+        moments(i, source)
+        lows_in(i, [to])
+
+    def halves_in(i, m):
+        if n > 1:
+            arrived(kinds[i][4].at[m, pl.ds(0, n - 1)], hr_r.at[i, m], other)
+
+    def half_on(i):
+        source, to = way_of(i)
+        half = kinds[i][4]
+        halves_in(i, source)
+        for j in from_fs:
+            send(half.at[source, j], half.at[source, j], hr_r.at[i, source], {"rep": to})
+
+    def squares(normed):
+        return jnp.sum(normed * normed, axis=0, keepdims=True).reshape(1, -1, 128).sum(axis=1)
+
+    reduced(1)
+    square_o = squares(moments(1, k))
+    share(1)
+    if ahead and n > 2:
+        w_step(2)
+    if across:
+        low_on(1)
+    reduced(0)
+    square_q = squares(moments(0, k))
+    tz[me] = square_q + square_o
+
+    everyone(lambda where: remote(tz.at[me], tz.at[me], tz_s, tz_r, where).start())
+    share(0)
     if ahead:
-        for copy in load_weights:
-            copy.wait()
-        for j in fs_peers:
-            send(wqv.at[first, cols(k, quarter_q)], early.at[f], we_r, {"fs": j})
+        for d in range(3, n):
+            w_step(d)
     spread_half(1)
-    gathered_moments(1)
     spread_half(0)
     if not ahead:
         for copy in load_weights:
             copy.wait()
+    if across:
+        low_on(0)
     others = tz.at[pl.ds(0, total - 1)]
     remote(others, others, tz_s, tz_r, other).wait_recv()
     scale = lax.rsqrt(jnp.sum(jnp.sum(tz[...], axis=0), axis=-1, keepdims=True) / entries + mean_eps)
@@ -402,47 +457,48 @@
         new[:, at] = fresh
         copy[cols(f, rows), at] = fresh.astype(BF16)
 
-    chunks = [(i, p) for p in range(parts) for i in range(2)]
+    chunks = [(i, start, size, bool(extra)) for start, size, extra in layout for i in range(2)]
     along_fs = [0] * len(chunks)
-    if across and ahead:
-        for at, c in enumerate(extras, 1):
+    if across:
+        for at, c in enumerate((c for c, v in enumerate(chunks) if v[3]), 1):
             along_fs[c] = at
 
     def block_of(c, j, m):
-        i, p = chunks[c]
-        copy, rows, width = outs[i][6], outs[i][7], outs[i][1]
-        return copy.at[cols(j * parts + p, rows // parts), cols(m, width)]
+        i, start, size, _ = chunks[c]
+        copy, rows, width, unit = outs[i][6], outs[i][7], outs[i][1], (unit_q, unit_o)[i]
+        return copy.at[pl.ds(pl.multiple_of(j * rows + start * unit, unit), size * unit), cols(m, width)]
 
     def spread(c, j, has=None, counted=True):
         i = chunks[c][0]
         block = block_of(c, j, k)
         for m in targets:
-            final = not across or (m is near) == (i == 1)
+            final = not across or bool(along_fs[c]) or (m is near) == (i == 1)
             send(block, block, late_r if final else cr_r.at[c, j], {"rep": m}, has, counted, 1)
 
     for i in range(2):
         weights(i, k)
-        for c, (kind, p) in enumerate(chunks):
-            if kind == i and not (ahead and c == 0):
+        for c in range(len(chunks)):
+            if chunks[c][0] == i and not (ahead and c == 0):
                 block = block_of(c, f, k)
                 for cond, to, way in outward:
                     send_line(1, block, block, cz_r.at[c, f], {"fs": to}, cond, way == 0)
     if ahead:
-        arrived(early.at[pl.ds(0, n - 1)], we_r, other)
         block = halfq[k].reshape(rank, quarter_q)
         for j in from_fs:
             moved = scale * jnp.dot(allq[j, first], block, preferred_element_type=F32)
-            cpq[cols(j * parts, early_rows), cols(k, quarter_q)] = (early[j] - learn_rate * moved).astype(BF16)
+            rows = pl.ds(pl.multiple_of(j * rows_q, rows_q), early_rows)
+            cpq[rows, cols(k, quarter_q)] = (early[j] - learn_rate * moved).astype(BF16)
             spread(0, j)
 
     def relay(d):
-        for c, (i, p) in enumerate(chunks):
-            source, to = (near, far) if i == 0 else (far, near)
+        for c in range(len(chunks)):
+            if along_fs[c]:
+                continue
+            source, to = (near, far) if chunks[c][0] == 0 else (far, near)
             for has, j, on, onward, way in sides(d):
                 block = block_of(c, j, source)
                 arrived(block, cr_r.at[c, j], {"rep": source}, has)
-                if not along_fs[c]:
-                    send(block, block, late_r, {"rep": to}, has, way == 0, 2)
+                send(block, block, late_r, {"rep": to}, has, way == 0, 2)
 
     def extra(d):
         for c in range(len(chunks)):
@@ -453,20 +509,24 @@
                     arrived(block, ex_r.at[at, j], {"fs": j}, has)
                     send_line(0, block, block, ex_r.at[at, j], {"fs": onward}, on)
 
-    def rest_of_weights():
-        gathered_moments(0)
-        for m in [beyond, near, far] if across else from_rep:
+    def more_weights(peers):
+        for m in peers:
             for i in range(2):
-                if n > 1:
-                    arrived(kinds[i][4].at[m, pl.ds(0, n - 1)], hr_r.at[i, m], other)
+                if not across or m is beyond:
+                    lows_in(i, [m])
+                if not across or m is not way_of(i)[0]:
+                    halves_in(i, m)
                 weights(i, m)
-            if across and m is beyond:
-                for c in range(len(chunks)):
-                    if along_fs[c]:
-                        block = block_of(c, f, beyond)
-                        for cond, to, way in outward:
-                            send_line(0, block, block, ex_r.at[along_fs[c] - 1, f], {"fs": to}, cond, way == 0)
-
+
+    def extras_out():
+        for c in range(len(chunks)):
+            if along_fs[c]:
+                block = block_of(c, f, beyond)
+                for cond, to, way in outward:
+                    send_line(0, block, block, ex_r.at[along_fs[c] - 1, f], {"fs": to}, cond, way == 0)
+
+    if across:
+        half_on(1)
     for d in range(1, n):
         for c in range(len(chunks)):
             if ahead and c == 0:
@@ -476,20 +536,27 @@
                 arrived(block, cz_r.at[c, j], {"fs": j}, has)
                 send_line(1, block, block, cz_r.at[c, j], {"fs": onward}, on)
                 spread(c, j, has, way == 0)
+            if across and d == 1 and c == min(3, len(chunks) - 1):
+                half_on(0)
+            if across and d == min(2, n - 1) and c == min(3, len(chunks) - 1):
+                more_weights([beyond])
+                extras_out()
         if d == 1:
-            rest_of_weights()
+            more_weights([near, far] if across else from_rep)
         if across and d > 1:
             relay(d - 1)
             extra(d - 1)
     if n == 1:
-        rest_of_weights()
+        if across:
+            half_on(0)
+        more_weights([near, far, beyond] if across else from_rep)
     if across and n > 1:
         relay(n - 1)
         extra(n - 1)
     if n > 1:
         count = 0
         for c in range(len(chunks)):
-            times = r - 1 if not across else 1 if along_fs[c] else 2
+            times = r - 1 if not across else 2
             count += (n - 1) * times * size_of(block_of(c, f, k))
         drain(count, late_r, False)
     for g, count in enumerate(bulk):
@@ -527,17 +594,21 @@
         low_rows = fq.shape[0]
         quarter_q, quarter_o = fq.shape[1] // r, fo.shape[1] // r
         entries = rank * (fq.shape[1] + fo.shape[1]) * tp
-        parts = 4 if n <= 8 else 1
+        if r == 4 and 1 < n <= 8:
+            units, layout = 8, ((0, 2, 0), (2, 2, 0), (4, 1, 0), (5, 1, 1), (6, 2, 1))
+        else:
+            units, layout = 1, ((0, 1, 0),)
         xparts = qparts = 2
-        ahead = r == 4 and parts == 4 and n > 1
-        extras = (5, 6, 7)
+        ahead = units > 1
+        pieces_of = 2 * len(layout)
+        extras = max(1, sum(2 * v[2] for v in layout))
         total = n * r * tp
         shape = jax.ShapeDtypeStruct
         like = lambda v: shape(v.shape, v.dtype)
         vmem = lambda v: pltpu.VMEM(v.shape, v.dtype)
         dma = pltpu.SemaphoreType.DMA
         made = pl.pallas_call(
-            functools.partial(kernel, n, r, tp, entries, parts, xparts, qparts, ahead, extras),
+            functools.partial(kernel, n, r, tp, entries, layout, units, xparts, qparts, ahead),
             out_shape=(
                 like(wq), like(wo), like(wq), like(wo), like(fq), like(sq), like(fo), like(so),
                 shape((n * wq.shape[0], wq.shape[1]), BF16),
@@ -563,11 +634,11 @@
                 pltpu.VMEM((r, n, low_rows, quarter_q), BF16),
                 pltpu.VMEM((r, n, low_rows, quarter_o), BF16),
                 pltpu.VMEM((total, 1, 128), F32),
-                pltpu.VMEM((n, wq.shape[0] // parts, quarter_q) if ahead else (8, 128), F32),
+                pltpu.VMEM((n, wq.shape[0] // units * layout[0][1], quarter_q) if ahead else (8, 128), F32),
                 dma((14,)), dma((8,)), dma((2,)),
                 dma((n,)), dma((qparts, n)), dma((1, max(r, 4))), dma((xparts, max(r, 4))),
-                dma((2,)), dma((2,)), dma((2,)), dma((2,)), dma((2,)), dma((2,)), dma((2,)), dma((2, r)),
-                dma(()), dma(()), dma((2 * parts, n)), dma((2 * parts, n)), dma(()), dma((len(extras), n)), dma(()),
+                dma((2,)), dma((2,)), dma((2,)), dma((2,)), dma((2,)), dma((2, r)), dma((2,)), dma((2, r)),
+                dma(()), dma(()), dma((pieces_of, n)), dma((pieces_of, n)), dma(()), dma((extras, n)), dma((n,)),
             ],
             compiler_params=pltpu.CompilerParams(collective_id=0, has_side_effects=True, vmem_limit_bytes=24 * 2**20),
         )(*(pltpu.with_memory_space_constraint(v, pltpu.HBM) for v in args))

time: 72.8 us -> 71.2 us (0.978)
  Pallas kernels: 71.9 us -> 70.4 us
    pallas_call x1, Pallas kernels: 68.1 us -> 66.6 us  [local(): pl.pallas_call(functools.partial(kernel, n, r, tp, entries, layout, units...]
where the time goes in v4:
time: 71.2 us; the launch traced here: 71.1 us
  Pallas kernels  70.4 us (99%)
    pallas_call x1, Pallas kernels, local(): pl.pallas_call(functools.partial(kernel, n, r, tp, entries, layout, units...  66.6 us
    pallas_call x1, Pallas kernels, local(): pl.pallas_call(functools.partial(place, pieces), out_shape=tuple((like(v)...  3.82 us

profile of v4, /device:TPU:0, one launch (start us, length us, event | category | flops | bytes accessed | tf_op | source)
XLA Modules:
  0.0 71.1 jit_solution(9735244373759542111)
XLA Ops:
  0.6 66.6 %shard_map.195 = (f32[512,512]{1,0:T(8,128)S(1)}, f32[256,1024]{1,0:T(8,128)S(1)}, f32[512,512]{1,0:T(8,128)S(1)}, f32[256,1024]{1,0:T(8,128)S(1)}, f32[64,512]{...) custom-call(bf16[128,2048]{1,0:T(8,128)(2,1)} %x_h.1, ...), custom_call_target="tpu_custom_call" | custom-call | tf_op jit(solution)/shard_map/pallas_call | solution.py:610
  67.2 3.8 %shard_map.196 = (f32[512,512]{1,0:T(8,128)}, f32[256,1024]{1,0:T(8,128)}, f32[512,512]{1,0:T(8,128)}, f32[256,1024]{1,0:T(8,128)}, f32[64,512]{1,0:T(8,128)}, /...) custom-call(f32[512,512]{1,0:T(8,128)S(1)} %get-tuple-element.20.ref, ...), custom_call_target="tpu_custom_call" | custom-call | tf_op jit(solution)/shard_map/pallas_call | solution.py:646

commit v5 on v4

--- a/solution.py
+++ b/solution.py
@@ -24,7 +24,7 @@
     x_h, qc_h, a_h, oc_h, pq_h, po_h, wq_h, wo_h, fq_h, sq_h, fo_h, so_h,
     nwq, nwo, stq, sto, nfq, nsq, nfo, nso, cpq, cpo,
     allq, allo, allx, alla, qcv, ocv, allqc, alloc, wqv, wov, fqv, sqv, fov, sov,
-    sbq, sbo, r2q, r2o, lowgq, lowgo, halfq, halfo, tz, early,
+    sbq, sbo, r2q, r2o, lowgq, lowgo, halfq, halfo, tz, early, ahead_raw,
     ld, gone, line_s, po_r, pq_r, ar_r, xr_r, pt_r, at_r, xt_r, cr1_r, r2_r, lg_r, hz_r, hr_r,
     tz_s, tz_r, cz_r, cr_r, late_r, ex_r, we_r,
 ):
@@ -69,7 +69,7 @@
 
     row_bytes = cpq.shape[1] * 2
     limit = cpq.shape[0] * row_bytes
-    bulk = [0, 0, 0, 0]
+    bulk = [0] * 5
 
     def size_of(ref):
         return math.prod(ref.shape) * jnp.dtype(ref.dtype).itemsize
@@ -122,7 +122,14 @@
                     if a or b or c:
                         action({"fs": fs[a], "rep": rep[b], "tp": 1 - t if c else t})
 
-    everyone(lambda where: pl.semaphore_signal(barrier, inc=1, device_id=where, device_id_type=MESH))
+    def greet(where, cond=None):
+        run(cond, lambda: pl.semaphore_signal(barrier, inc=1, device_id=where, device_id_type=MESH))
+
+    for j in rep_peers:
+        greet({"rep": j})
+    greet(other)
+    greet({"fs": lax.rem(f + 1, n)}, f < n - 1)
+    greet({"fs": lax.rem(f + n - 1, n)}, f > 0)
 
     loads = []
 
@@ -146,7 +153,8 @@
     load_po.wait()
     load_a.wait()
     load_oc.wait()
-    pl.semaphore_wait(barrier, total - 1)
+    for v in range(n):
+        run(f == v, functools.partial(pl.semaphore_wait, barrier, r + (v > 0) + (v < n - 1)))
 
     def sides(d):
         return (
@@ -431,8 +439,32 @@
     if ahead:
         for d in range(3, n):
             w_step(d)
+    outs = (
+        (None, quarter_q, halfq, wqv, nwq, stq, cpq, rows_q, allq),
+        (None, quarter_o, halfo, wov, nwo, sto, cpo, rows_o, allo),
+    )
+
+    def raw_step(i, index):
+        _, width, half, old, new, step, copy, rows, proj = outs[i]
+        return jnp.dot(proj[f], half[index].reshape(rank, width), preferred_element_type=F32)
+
+    def weights(i, index, raw):
+        _, width, half, old, new, step, copy, rows, proj = outs[i]
+        at = cols(index, width)
+        moved = scale * raw
+        fresh = old[:, at] - learn_rate * moved
+        step[:, at] = moved
+        new[:, at] = fresh
+        copy[cols(f, rows), at] = fresh.astype(BF16)
+
     spread_half(1)
+    sto[:, cols(k, quarter_o)] = raw_step(1, k)
     spread_half(0)
+    stq[:, cols(k, quarter_q)] = raw_step(0, k)
+    if ahead:
+        for d in range(1, n):
+            j = lax.rem(f + d, n)
+            ahead_raw[j] = jnp.dot(allq[j, first], halfq[k].reshape(rank, quarter_q), preferred_element_type=F32)
     if not ahead:
         for copy in load_weights:
             copy.wait()
@@ -442,26 +474,13 @@
     remote(others, others, tz_s, tz_r, other).wait_recv()
     scale = lax.rsqrt(jnp.sum(jnp.sum(tz[...], axis=0), axis=-1, keepdims=True) / entries + mean_eps)
 
-    outs = (
-        (None, quarter_q, halfq, wqv, nwq, stq, cpq, rows_q, allq),
-        (None, quarter_o, halfo, wov, nwo, sto, cpo, rows_o, allo),
-    )
-
-    def weights(i, index):
-        _, width, half, old, new, step, copy, rows, proj = outs[i]
-        at = cols(index, width)
-        block = half[index].reshape(rank, width)
-        moved = scale * jnp.dot(proj[f], block, preferred_element_type=F32)
-        fresh = old[:, at] - learn_rate * moved
-        step[:, at] = moved
-        new[:, at] = fresh
-        copy[cols(f, rows), at] = fresh.astype(BF16)
-
-    chunks = [(i, start, size, bool(extra)) for start, size, extra in layout for i in range(2)]
+    chunks = [(i, start, size, extra[i]) for start, size, extra in layout for i in range(2)]
     along_fs = [0] * len(chunks)
     if across:
         for at, c in enumerate((c for c, v in enumerate(chunks) if v[3]), 1):
             along_fs[c] = at
+
+    relayed = [sum(not v for v in along_fs[:c]) for c in range(len(chunks))]
 
     def block_of(c, j, m):
         i, start, size, _ = chunks[c]
@@ -473,19 +492,18 @@
         block = block_of(c, j, k)
         for m in targets:
             final = not across or bool(along_fs[c]) or (m is near) == (i == 1)
-            send(block, block, late_r if final else cr_r.at[c, j], {"rep": m}, has, counted, 1)
+            send(block, block, late_r if final else cr_r.at[relayed[c], j], {"rep": m}, has, counted, 1)
 
     for i in range(2):
-        weights(i, k)
+        weights(i, k, (stq, sto)[i][:, cols(k, (quarter_q, quarter_o)[i])])
         for c in range(len(chunks)):
             if chunks[c][0] == i and not (ahead and c == 0):
                 block = block_of(c, f, k)
                 for cond, to, way in outward:
-                    send_line(1, block, block, cz_r.at[c, f], {"fs": to}, cond, way == 0)
+                    send_line(1, block, block, cz_r.at[c - ahead, f], {"fs": to}, cond, way == 0)
     if ahead:
-        block = halfq[k].reshape(rank, quarter_q)
         for j in from_fs:
-            moved = scale * jnp.dot(allq[j, first], block, preferred_element_type=F32)
+            moved = scale * ahead_raw[j]
             rows = pl.ds(pl.multiple_of(j * rows_q, rows_q), early_rows)
             cpq[rows, cols(k, quarter_q)] = (early[j] - learn_rate * moved).astype(BF16)
             spread(0, j)
@@ -497,7 +515,7 @@
             source, to = (near, far) if chunks[c][0] == 0 else (far, near)
             for has, j, on, onward, way in sides(d):
                 block = block_of(c, j, source)
-                arrived(block, cr_r.at[c, j], {"rep": source}, has)
+                arrived(block, cr_r.at[relayed[c], j], {"rep": source}, has)
                 send(block, block, late_r, {"rep": to}, has, way == 0, 2)
 
     def extra(d):
@@ -516,7 +534,7 @@
                     lows_in(i, [m])
                 if not across or m is not way_of(i)[0]:
                     halves_in(i, m)
-                weights(i, m)
+                weights(i, m, raw_step(i, m))
 
     def extras_out():
         for c in range(len(chunks)):
@@ -533,8 +551,8 @@
                 continue
             for has, j, on, onward, way in sides(d):
                 block = block_of(c, j, k)
-                arrived(block, cz_r.at[c, j], {"fs": j}, has)
-                send_line(1, block, block, cz_r.at[c, j], {"fs": onward}, on)
+                arrived(block, cz_r.at[c - ahead, j], {"fs": j}, has)
+                send_line(1, block, block, cz_r.at[c - ahead, j], {"fs": onward}, on)
                 spread(c, j, has, way == 0)
             if across and d == 1 and c == min(3, len(chunks) - 1):
                 half_on(0)
@@ -595,13 +613,14 @@
         quarter_q, quarter_o = fq.shape[1] // r, fo.shape[1] // r
         entries = rank * (fq.shape[1] + fo.shape[1]) * tp
         if r == 4 and 1 < n <= 8:
-            units, layout = 8, ((0, 2, 0), (2, 2, 0), (4, 1, 0), (5, 1, 1), (6, 2, 1))
+            units, layout = 8, ((0, 2, (0, 0)), (2, 2, (0, 0)), (4, 1, (0, 1)), (5, 3, (1, 1)))
         else:
-            units, layout = 1, ((0, 1, 0),)
+            units, layout = 1, ((0, 1, (0, 0)),)
         xparts = qparts = 2
         ahead = units > 1
         pieces_of = 2 * len(layout)
-        extras = max(1, sum(2 * v[2] for v in layout))
+        relays = pieces_of - sum(sum(v[2]) for v in layout)
+        extras = max(1, sum(sum(v[2]) for v in layout))
         total = n * r * tp
         shape = jax.ShapeDtypeStruct
         like = lambda v: shape(v.shape, v.dtype)
@@ -635,14 +654,15 @@
                 pltpu.VMEM((r, n, low_rows, quarter_o), BF16),
                 pltpu.VMEM((total, 1, 128), F32),
                 pltpu.VMEM((n, wq.shape[0] // units * layout[0][1], quarter_q) if ahead else (8, 128), F32),
-                dma((14,)), dma((8,)), dma((2,)),
+                pltpu.VMEM((n, wq.shape[0] // units * layout[0][1], quarter_q) if ahead else (8, 128), F32),
+                dma((14,)), dma((9,)), dma((2,)),
                 dma((n,)), dma((qparts, n)), dma((1, max(r, 4))), dma((xparts, max(r, 4))),
                 dma((2,)), dma((2,)), dma((2,)), dma((2,)), dma((2,)), dma((2, r)), dma((2,)), dma((2, r)),
-                dma(()), dma(()), dma((pieces_of, n)), dma((pieces_of, n)), dma(()), dma((extras, n)), dma((n,)),
+                dma(()), dma(()), dma((pieces_of - ahead, n)), dma((relays, n)), dma(()), dma((extras, n)), dma((n,)),
             ],
             compiler_params=pltpu.CompilerParams(collective_id=0, has_side_effects=True, vmem_limit_bytes=24 * 2**20),
         )(*(pltpu.with_memory_space_constraint(v, pltpu.HBM) for v in args))
-        pieces = tuple(max(1, min(8, v.size * v.dtype.itemsize // 2**18)) for v in made)
+        pieces = tuple(max(1, min(8, v.size * v.dtype.itemsize // 2**20)) for v in made)
         return pl.pallas_call(
             functools.partial(place, pieces),
             out_shape=tuple(like(v) for v in made),

time: 71.2 us -> 68.6 us (0.963)
  Pallas kernels: 70.4 us -> 67.8 us
    pallas_call x1, Pallas kernels: 66.6 us -> 64.2 us  [local(): pl.pallas_call(functools.partial(kernel, n, r, tp, entries, layout, units...]
where the time goes in v5:
time: 68.6 us; the launch traced here: 68.5 us
  Pallas kernels  67.8 us (99%)
    pallas_call x1, Pallas kernels, local(): pl.pallas_call(functools.partial(kernel, n, r, tp, entries, layout, units...  64.2 us
    pallas_call x1, Pallas kernels, local(): pl.pallas_call(functools.partial(place, pieces), out_shape=tuple((like(v)...  3.65 us

profile of v5, /device:TPU:0, one launch (start us, length us, event | category | flops | bytes accessed | tf_op | source)
XLA Modules:
  0.0 68.5 jit_solution(17253501327907259506)
XLA Ops:
  0.6 64.2 %shard_map.195 = (f32[512,512]{1,0:T(8,128)S(1)}, f32[256,1024]{1,0:T(8,128)S(1)}, f32[512,512]{1,0:T(8,128)S(1)}, f32[256,1024]{1,0:T(8,128)S(1)}, f32[64,512]{...) custom-call(bf16[128,2048]{1,0:T(8,128)(2,1)} %x_h.1, ...), custom_call_target="tpu_custom_call" | custom-call | tf_op jit(solution)/shard_map/pallas_call | solution.py:629
  64.8 3.6 %shard_map.196 = (f32[512,512]{1,0:T(8,128)}, f32[256,1024]{1,0:T(8,128)}, f32[512,512]{1,0:T(8,128)}, f32[256,1024]{1,0:T(8,128)}, f32[64,512]{1,0:T(8,128)}, /...) custom-call(f32[512,512]{1,0:T(8,128)S(1)} %get-tuple-element.20.ref, ...), custom_call_target="tpu_custom_call" | custom-call | tf_op jit(solution)/shard_map/pallas_call | solution.py:666

commit v6 on v5

--- a/solution.py
+++ b/solution.py
@@ -25,7 +25,7 @@
     nwq, nwo, stq, sto, nfq, nsq, nfo, nso, cpq, cpo,
     allq, allo, allx, alla, qcv, ocv, allqc, alloc, wqv, wov, fqv, sqv, fov, sov,
     sbq, sbo, r2q, r2o, lowgq, lowgo, halfq, halfo, tz, early, ahead_raw,
-    ld, gone, line_s, po_r, pq_r, ar_r, xr_r, pt_r, at_r, xt_r, cr1_r, r2_r, lg_r, hz_r, hr_r,
+    ld, gone, line_s, pt_r, at_r, xt_r, cr1_r, r2_r, lg_r, hz_r, hr_r,
     tz_s, tz_r, cz_r, cr_r, late_r, ex_r, we_r,
 ):
     f, k, t = lax.axis_index("fs"), lax.axis_index("rep"), lax.axis_index("tp")
@@ -104,6 +104,8 @@
     def cols(index, width):
         return pl.ds(pl.multiple_of(index * width, width), width)
 
+    pq_r, xr_r = cz_r.at[pl.ds(0, qparts)], cz_r.at[pl.ds(qparts, xparts)]
+    po_r, ar_r = cz_r.at[qparts + xparts], cz_r.at[pl.ds(qparts + xparts + 1, 1)]
     barrier = pltpu.get_barrier_semaphore()
 
     def everyone(action):
@@ -426,10 +428,10 @@
     reduced(1)
     square_o = squares(moments(1, k))
     share(1)
+    if across:
+        low_on(1)
     if ahead and n > 2:
         w_step(2)
-    if across:
-        low_on(1)
     reduced(0)
     square_q = squares(moments(0, k))
     tz[me] = square_q + square_o
@@ -613,7 +615,7 @@
         quarter_q, quarter_o = fq.shape[1] // r, fo.shape[1] // r
         entries = rank * (fq.shape[1] + fo.shape[1]) * tp
         if r == 4 and 1 < n <= 8:
-            units, layout = 8, ((0, 2, (0, 0)), (2, 2, (0, 0)), (4, 1, (0, 1)), (5, 3, (1, 1)))
+            units, layout = 8, ((0, 2, (0, 0)), (2, 2, (0, 0)), (4, 4, (1, 1)))
         else:
             units, layout = 1, ((0, 1, (0, 0)),)
         xparts = qparts = 2
@@ -656,9 +658,8 @@
                 pltpu.VMEM((n, wq.shape[0] // units * layout[0][1], quarter_q) if ahead else (8, 128), F32),
                 pltpu.VMEM((n, wq.shape[0] // units * layout[0][1], quarter_q) if ahead else (8, 128), F32),
                 dma((14,)), dma((9,)), dma((2,)),
-                dma((n,)), dma((qparts, n)), dma((1, max(r, 4))), dma((xparts, max(r, 4))),
-                dma((2,)), dma((2,)), dma((2,)), dma((2,)), dma((2,)), dma((2, r)), dma((2,)), dma((2, r)),
-                dma(()), dma(()), dma((pieces_of - ahead, n)), dma((relays, n)), dma(()), dma((extras, n)), dma((n,)),
+                                dma((2,)), dma((2,)), dma((2,)), dma((2,)), dma((2,)), dma((2, r)), dma((2,)), dma((2, r)),
+                dma(()), dma(()), dma((max(pieces_of - ahead, qparts + xparts + 2), max(n, r, 4))), dma((relays, n)), dma(()), dma((extras, n)), dma((n,)),
             ],
             compiler_params=pltpu.CompilerParams(collective_id=0, has_side_effects=True, vmem_limit_bytes=24 * 2**20),
         )(*(pltpu.with_memory_space_constraint(v, pltpu.HBM) for v in args))

time: 68.6 us -> 68.4 us (level)
  no operation moved by 1% of the time
where the time goes in v6:
time: 68.4 us; the launch traced here: 68.2 us
  Pallas kernels  67.6 us (99%)
    pallas_call x1, Pallas kernels, local(): pl.pallas_call(functools.partial(kernel, n, r, tp, entries, layout, units...  63.9 us
    pallas_call x1, Pallas kernels, local(): pl.pallas_call(functools.partial(place, pieces), out_shape=tuple((like(v)...  3.65 us

profile of v6, /device:TPU:0, one launch (start us, length us, event | category | flops | bytes accessed | tf_op | source)
XLA Modules:
  0.0 68.2 jit_solution(15630360167557338592)
XLA Ops:
  0.6 63.9 %shard_map.195 = (f32[512,512]{1,0:T(8,128)S(1)}, f32[256,1024]{1,0:T(8,128)S(1)}, f32[512,512]{1,0:T(8,128)S(1)}, f32[256,1024]{1,0:T(8,128)S(1)}, f32[64,512]{...) custom-call(bf16[128,2048]{1,0:T(8,128)(2,1)} %x_h.1, ...), custom_call_target="tpu_custom_call" | custom-call | tf_op jit(solution)/shard_map/pallas_call | solution.py:631
  64.6 3.6 %shard_map.196 = (f32[512,512]{1,0:T(8,128)}, f32[256,1024]{1,0:T(8,128)}, f32[512,512]{1,0:T(8,128)}, f32[256,1024]{1,0:T(8,128)}, f32[64,512]{1,0:T(8,128)}, /...) custom-call(f32[512,512]{1,0:T(8,128)S(1)} %get-tuple-element.20.ref, ...), custom_call_target="tpu_custom_call" | custom-call | tf_op jit(solution)/shard_map/pallas_call | solution.py:667

commit v7 on v6

--- a/solution.py
+++ b/solution.py
@@ -498,11 +498,10 @@
 
     for i in range(2):
         weights(i, k, (stq, sto)[i][:, cols(k, (quarter_q, quarter_o)[i])])
-        for c in range(len(chunks)):
-            if chunks[c][0] == i and not (ahead and c == 0):
-                block = block_of(c, f, k)
-                for cond, to, way in outward:
-                    send_line(1, block, block, cz_r.at[c - ahead, f], {"fs": to}, cond, way == 0)
+    for c in range(int(ahead), len(chunks)):
+        block = block_of(c, f, k)
+        for cond, to, way in outward:
+            send_line(1, block, block, cz_r.at[c - ahead, f], {"fs": to}, cond, way == 0)
     if ahead:
         for j in from_fs:
             moved = scale * ahead_raw[j]
@@ -510,9 +509,15 @@
             cpq[rows, cols(k, quarter_q)] = (early[j] - learn_rate * moved).astype(BF16)
             spread(0, j)
 
-    def relay(d):
-        for c in range(len(chunks)):
-            if along_fs[c]:
+    def relay_early():
+        block_q = [block_of(0, j, near) for j in from_fs]
+        for j, block in zip(from_fs, block_q):
+            arrived(block, cr_r.at[0, j], {"rep": near})
+            send(block, block, late_r, {"rep": far}, None, True, 2)
+
+    def relay(d, some=None):
+        for c in range(len(chunks)) if some is None else some:
+            if along_fs[c] or (ahead and c == 0):
                 continue
             source, to = (near, far) if chunks[c][0] == 0 else (far, near)
             for has, j, on, onward, way in sides(d):
@@ -556,15 +561,19 @@
                 arrived(block, cz_r.at[c - ahead, j], {"fs": j}, has)
                 send_line(1, block, block, cz_r.at[c - ahead, j], {"fs": onward}, on)
                 spread(c, j, has, way == 0)
+            if across and d > 2:
+                relay(d - 1, [c])
             if across and d == 1 and c == min(3, len(chunks) - 1):
                 half_on(0)
             if across and d == min(2, n - 1) and c == min(3, len(chunks) - 1):
                 more_weights([beyond])
                 extras_out()
         if d == 1:
+            if across and ahead:
+                relay_early()
             more_weights([near, far] if across else from_rep)
         if across and d > 1:
-            relay(d - 1)
+            relay(d - 1, None if d == 2 else [])
             extra(d - 1)
     if n == 1:
         if across:

time: 68.4 us -> 67.7 us (0.990)
  Pallas kernels: 67.6 us -> 66.9 us
    pallas_call x1, Pallas kernels: 63.9 us -> 63.2 us  [local(): pl.pallas_call(functools.partial(kernel, n, r, tp, entries, layout, units...]
where the time goes in v7:
time: 67.7 us; the launch traced here: 67.5 us
  Pallas kernels  66.9 us (99%)
    pallas_call x1, Pallas kernels, local(): pl.pallas_call(functools.partial(kernel, n, r, tp, entries, layout, units...  63.2 us
    pallas_call x1, Pallas kernels, local(): pl.pallas_call(functools.partial(place, pieces), out_shape=tuple((like(v)...  3.65 us

profile of v7, /device:TPU:0, one launch (start us, length us, event | category | flops | bytes accessed | tf_op | source)
XLA Modules:
  0.0 67.5 jit_solution(11743573976803942189)
XLA Ops:
  0.6 63.2 %shard_map.195 = (f32[512,512]{1,0:T(8,128)S(1)}, f32[256,1024]{1,0:T(8,128)S(1)}, f32[512,512]{1,0:T(8,128)S(1)}, f32[256,1024]{1,0:T(8,128)S(1)}, f32[64,512]{...) custom-call(bf16[128,2048]{1,0:T(8,128)(2,1)} %x_h.1, ...), custom_call_target="tpu_custom_call" | custom-call | tf_op jit(solution)/shard_map/pallas_call | solution.py:640
  63.9 3.6 %shard_map.196 = (f32[512,512]{1,0:T(8,128)}, f32[256,1024]{1,0:T(8,128)}, f32[512,512]{1,0:T(8,128)}, f32[256,1024]{1,0:T(8,128)}, f32[64,512]{1,0:T(8,128)}, /...) custom-call(f32[512,512]{1,0:T(8,128)S(1)} %get-tuple-element.20.ref, ...), custom_call_target="tpu_custom_call" | custom-call | tf_op jit(solution)/shard_map/pallas_call | solution.py:676

commit v8 on v7

--- a/solution.py
+++ b/solution.py
@@ -265,10 +265,10 @@
         pass_on(*a_args)
     load_qc.wait()
     load_x.wait()
+    for c in range(xparts):
+        post(allx, x_rows(c, t), xr_r, (c,), slots)
     for j, d in rep_slots:
         send(qcv.at[:, cols(j, quarter_q)], allqc.at[deposit[d]], cr1_r.at[0], {"rep": j})
-    for c in range(xparts):
-        post(allx, x_rows(c, t), xr_r, (c,), slots)
     if n > 1:
         pq_step(1, 0)
     if n > 2:

time: 67.7 us -> 67.9 us (level)
  no operation moved by 1% of the time
where the time goes in v8:
time: 67.9 us; the launch traced here: 67.8 us
  Pallas kernels  67.1 us (99%)
    pallas_call x1, Pallas kernels, local(): pl.pallas_call(functools.partial(kernel, n, r, tp, entries, layout, units...  63.5 us
    pallas_call x1, Pallas kernels, local(): pl.pallas_call(functools.partial(place, pieces), out_shape=tuple((like(v)...  3.65 us

profile of v8, /device:TPU:0, one launch (start us, length us, event | category | flops | bytes accessed | tf_op | source)
XLA Modules:
  0.0 67.8 jit_solution(10260128579370509374)
XLA Ops:
  0.6 63.5 %shard_map.195 = (f32[512,512]{1,0:T(8,128)S(1)}, f32[256,1024]{1,0:T(8,128)S(1)}, f32[512,512]{1,0:T(8,128)S(1)}, f32[256,1024]{1,0:T(8,128)S(1)}, f32[64,512]{...) custom-call(bf16[128,2048]{1,0:T(8,128)(2,1)} %x_h.1, ...), custom_call_target="tpu_custom_call" | custom-call | tf_op jit(solution)/shard_map/pallas_call | solution.py:640
  64.1 3.6 %shard_map.196 = (f32[512,512]{1,0:T(8,128)}, f32[256,1024]{1,0:T(8,128)}, f32[512,512]{1,0:T(8,128)}, f32[256,1024]{1,0:T(8,128)}, f32[64,512]{1,0:T(8,128)}, /...) custom-call(f32[512,512]{1,0:T(8,128)S(1)} %get-tuple-element.20.ref, ...), custom_call_target="tpu_custom_call" | custom-call | tf_op jit(solution)/shard_map/pallas_call | solution.py:676
